TPU v7x, 256 devices: a whole 4x4x8 slice. The times are simulated.
256 devices in a mesh: ep: 16 (over y, x), tp: 16 (over z, core).
Axes of the slice: x: 4, y: 4, z: 8, core: 2. Of those that a mesh axis runs over, the one named last changes fastest.
Arguments:
- stream: bfloat16 [131072, 1024], P(('ep', 'tp')), may hold values from -6 to 6
- norm_gain: float32 [1024], replicated, may hold values from 0.5 to 1.5
- gate_rows: bfloat16 [16, 1024, 1024], P('ep', 'tp'), may hold values from -0.1875 to 0.1875
- up_rows: bfloat16 [16, 1024, 1024], P('ep', 'tp'), may hold values from -0.1875 to 0.1875
- down_rows: bfloat16 [16, 1024, 1024], P('ep', 'tp'), may hold values from -0.1875 to 0.1875
- chosen: int32 [16, 16384], P('ep'), may hold values from 0 to 131071, as said below
- affinity: float32 [16, 16384], P('ep'), may hold values from 0.2 to 1
Outputs:
- mixed_out: bfloat16 [131072, 1024], P(('ep', 'tp'))
Inputs may be any that keep to these rules, and one draw needn't show every extreme that they name: Each row of chosen names 16384 different token numbers in increasing order. Among the 512 consecutive token numbers of any one device, an expert reads at most 128, and for every expert some device holds exactly 128 of its tokens.
All inputs are finite; a program needn't handle non-finite values.
Results may differ from a plain program's by a relative error of at most 0.008.
Values may be sent and summed in bfloat16 or wider, within the bound.
No kernel may reach another device: no remote copies, remote signals or barrier semaphores. Data moves between devices by JAX's collectives and lax.ppermute only.
A program may use at most 64 MiB of HBM per device.

v0:
```python
import functools

import jax
import jax.numpy as jnp
from jax import lax
from jax.experimental import pallas as pl
from jax.experimental.pallas import tpu as pltpu
from jax.sharding import PartitionSpec as P

epsilon = 1e-06
SIDE = 4
SMEM = pl.BlockSpec(memory_space=pltpu.SMEM)
VMEM = pl.BlockSpec(memory_space=pltpu.VMEM)


def wrap(value):
    return lax.rem(value + SIDE, SIDE)


def windows_kernel(block, slots, bounds_ref, list_ref, affinity_ref, rows_ref, weights_ref):
    listed = list_ref[...]
    lines = listed.shape[0]
    lane = lax.broadcasted_iota(jnp.int32, (1, slots), 1)
    for j in range(weights_ref.shape[0]):
        y, x = divmod(j, SIDE)
        bound = bounds_ref[j]
        start = jnp.sum((listed < bound).astype(jnp.int32))
        line, shift = start // slots, start % slots
        first = jnp.minimum(line, lines - 1)
        second = jnp.minimum(line + 1, lines - 1)
        back = lax.rem(slots - shift, slots)

        def window(ref):
            low = pltpu.roll(ref[pl.ds(first, 1), :], back, 1)
            high = pltpu.roll(ref[pl.ds(second, 1), :], back, 1)
            return jnp.where(lane < slots - shift, low, high)

        rows = window(list_ref) - bound
        rows = jnp.where((rows >= 0) & (rows < block), rows, -1)
        for t in range(SIDE):
            rows_ref[y * SIDE + (x + t) % SIDE, t : t + 1, :] = rows
            rows_ref[(y + t) % SIDE * SIDE + x, SIDE + t : SIDE + t + 1, :] = rows
        weights_ref[j : j + 1, :] = window(affinity_ref)


def windows(bounds, listed, affinity, block, slots):
    count = bounds.shape[0]
    return pl.pallas_call(
        functools.partial(windows_kernel, block, slots),
        in_specs=[SMEM, VMEM, VMEM],
        out_shape=(
            jax.ShapeDtypeStruct((count, 2 * SIDE, slots), jnp.int32),
            jax.ShapeDtypeStruct((count, slots), jnp.float32),
        ),
        cost_estimate=pl.CostEstimate(flops=8_000_000, bytes_accessed=150_000, transcendentals=0),
        name="windows",
    )(bounds, listed.reshape(-1, slots), affinity.reshape(-1, slots))


def prepare_kernel(stream_ref, gain_ref, gate_ref, up_ref, down_ref, low_ref, high_ref, piece_ref):
    values = stream_ref[...].astype(jnp.float32)
    inverse = lax.rsqrt(jnp.mean(values * values, axis=-1, keepdims=True) + epsilon)
    normed = (values * inverse * gain_ref[...]).astype(jnp.bfloat16)
    half = low_ref.shape[1]
    low_ref[...] = normed[:, :half]
    high_ref[...] = normed[:, half:]

    @pl.when(pl.program_id(0) == 0)
    def _():
        piece_ref[0:1] = gate_ref[...]
        piece_ref[1:2] = up_ref[...]
        piece_ref[2:3] = down_ref[...]


def prepare(stream, norm_gain, parts):
    rows, features = stream.shape
    step, half = rows // 2, features // 2
    part = pl.BlockSpec(parts[0].shape, lambda i: (0, 0, 0))
    piece = (3, *parts[0].shape[1:])
    return pl.pallas_call(
        prepare_kernel,
        grid=(2,),
        in_specs=[
            pl.BlockSpec((step, features), lambda i: (i, 0)),
            pl.BlockSpec((1, features), lambda i: (0, 0)),
            part,
            part,
            part,
        ],
        out_specs=(
            pl.BlockSpec((step, half), lambda i: (i, 0)),
            pl.BlockSpec((step, half), lambda i: (i, 0)),
            pl.BlockSpec(piece, lambda i: (0, 0, 0)),
        ),
        out_shape=(
            jax.ShapeDtypeStruct((rows, half), jnp.bfloat16),
            jax.ShapeDtypeStruct((rows, half), jnp.bfloat16),
            jax.ShapeDtypeStruct(piece, jnp.bfloat16),
        ),
        cost_estimate=pl.CostEstimate(flops=3_000_000, bytes_accessed=3 << 20, transcendentals=512),
        name="prepare",
    )(stream, norm_gain.reshape(1, features), *parts)


def pick_kernel(along_y, place_ref, rows_ref, *refs):
    sources, outs = refs[:SIDE], refs[SIDE:]
    y, x = place_ref[0], place_ref[1]
    tokens, slots = sources[0].shape[0], rows_ref.shape[2]
    token = lax.broadcasted_iota(jnp.int32, (slots, tokens), 1).astype(jnp.float32)
    columns = []
    for d in range(SIDE):
        e = wrap(y + d) * SIDE + x if along_y else y * SIDE + wrap(x + d)
        columns.append(rows_ref[e].astype(jnp.float32).T)
    for t in range(SIDE):
        k = t if along_y else SIDE + t
        chosen = jnp.concatenate(
            [jnp.where(column[:, k : k + 1] == token, 1.0, 0.0).astype(jnp.bfloat16) for column in columns]
        )
        rows = jnp.dot(chosen, sources[t][...], preferred_element_type=jnp.float32).astype(jnp.bfloat16)
        for d in range(SIDE):
            outs[d][t * slots : (t + 1) * slots, :] = rows[d * slots : (d + 1) * slots, :]


def pick(along_y, place, rows, sources):
    tokens, half = sources[0].shape
    slots = rows.shape[2]
    return pl.pallas_call(
        functools.partial(pick_kernel, along_y),
        in_specs=[SMEM] + [VMEM] * (1 + SIDE),
        out_shape=[jax.ShapeDtypeStruct((SIDE * slots, half), jnp.bfloat16)] * SIDE,
        cost_estimate=pl.CostEstimate(
            flops=2 * SIDE * SIDE * slots * tokens * half, bytes_accessed=4 << 20, transcendentals=0
        ),
        compiler_params=pltpu.CompilerParams(vmem_limit_bytes=12 << 20),
        name="pick_y" if along_y else "pick_x",
    )(place, rows, *sources)


def stack_kernel(*refs):
    out_ref, at = refs[-1], 0
    for piece in refs[:-1]:
        width = piece.shape[1]
        out_ref[:, at : at + width, :] = piece[...]
        at += width


def stack(pieces):
    return pl.pallas_call(
        stack_kernel,
        in_specs=[VMEM] * len(pieces),
        out_shape=jax.ShapeDtypeStruct(
            (3, sum(piece.shape[1] for piece in pieces), pieces[0].shape[2]), jnp.bfloat16
        ),
        cost_estimate=pl.CostEstimate(flops=1_000_000, bytes_accessed=4 << 20, transcendentals=0),
        compiler_params=pltpu.CompilerParams(vmem_limit_bytes=8 << 20),
    )(*pieces)


def assemble_kernel(*refs):
    pieces, outs = refs[:-3], refs[-3:]
    at = 0
    for piece in pieces:
        width = piece.shape[1]
        for j, out in enumerate(outs):
            out[at : at + width, :] = piece[j]
        at += width


def assemble(pieces):
    shape = jax.ShapeDtypeStruct((sum(piece.shape[1] for piece in pieces), pieces[0].shape[2]), jnp.bfloat16)
    return pl.pallas_call(
        assemble_kernel,
        in_specs=[VMEM] * len(pieces),
        out_shape=[shape] * 3,
        cost_estimate=pl.CostEstimate(flops=1_000_000, bytes_accessed=12 << 20, transcendentals=0),
        compiler_params=pltpu.CompilerParams(vmem_limit_bytes=16 << 20),
        name="assemble",
    )(*pieces)


STEPS = (
    ((2, 0), (2, 1), (2, 2), (2, 3), (0, 2), (1, 2), (3, 2), (1, 1)),
    ((1, 0), (1, 3), (0, 1), (3, 1), (3, 0), (3, 3), (0, 3), (0, 0)),
)
FINISHED = (
    (("low", 2), ("high", 2)),
    (("low", 1), ("high", 1), ("low", 3), ("high", 3), ("low", 0), ("high", 0)),
)


def members(piece):
    half, fixed = piece
    return [(fixed, k) if half == "low" else (k, fixed) for k in range(SIDE)]


def expert_kernel(number, names, place_ref, weights_ref, gate_ref, up_ref, down_ref, *refs):
    inputs_ref, result_ref, columns_ref = refs[-3:]
    ref = dict(zip(names, refs))
    blocks = STEPS[number]
    y, x = place_ref[0], place_ref[1]
    slots, half = weights_ref.shape[1], ref["in", "low", blocks[0][0]].shape[1]
    for k, (a, b) in enumerate(blocks):
        at = slice(k * slots, (k + 1) * slots)
        inputs_ref[at, :half] = ref["in", "low", a][b * slots : (b + 1) * slots, :]
        inputs_ref[at, half:] = ref["in", "high", b][a * slots : (a + 1) * slots, :]
        line = weights_ref[pl.ds(wrap(y - a) * SIDE + wrap(x - b), 1), :]
        columns_ref[at, :] = jnp.broadcast_to(line, (slots, slots)).T
    last = (((1,), (1,)), ((), ()))
    units = gate_ref.shape[0]
    width, rows = units // 4, SIDE * slots

    def work(i, carry):
        at = pl.ds(pl.multiple_of(i * rows, rows), rows)
        inputs = inputs_ref[at, :]
        hidden = []
        for f in range(0, units, width):
            gate_sum = lax.dot_general(inputs, gate_ref[f : f + width, :], last, preferred_element_type=jnp.float32)
            up_sum = lax.dot_general(inputs, up_ref[f : f + width, :], last, preferred_element_type=jnp.float32)
            hidden.append((gate_sum / (1.0 + jnp.exp(-gate_sum)) * up_sum).astype(jnp.bfloat16))
        result = jnp.dot(jnp.concatenate(hidden, 1), down_ref[...], preferred_element_type=jnp.float32)
        result_ref[at, :] = (result * columns_ref[at, :][:, :1]).astype(jnp.bfloat16)
        return carry

    lax.fori_loop(0, len(blocks) // SIDE, work, 0)

    def part(block, which):
        if block in blocks:
            k = blocks.index(block)
            cut = slice(0, half) if which == "low" else slice(half, 2 * half)
            return result_ref[k * slots : (k + 1) * slots, cut]
        step = next(n for n in range(number) if block in STEPS[n])
        k = STEPS[step].index(block)
        return ref["made", which, step][k * slots : (k + 1) * slots, :]

    for name in names:
        if name[0] == "out":
            for k, block in enumerate(members(name[1:])):
                ref[name][k * slots : (k + 1) * slots, :] = part(block, name[1])
        if name == ("made", name[1], number):
            for k, block in enumerate(blocks):
                ref[name][k * slots : (k + 1) * slots, :] = part(block, name[1])


def expert(number, place, weights, projections, low, high, made):
    slots, half = weights.shape[1], low[0].shape[1]
    features, units = 2 * half, projections[0].shape[0]
    piece_rows = SIDE * slots
    blocks = STEPS[number]
    total = len(blocks) * slots
    inputs = {("in", "low", a): low[a] for a, _ in blocks}
    inputs.update({("in", "high", b): high[b] for _, b in blocks})
    for piece in FINISHED[number]:
        for block in members(piece):
            step = next(n for n in range(len(STEPS)) if block in STEPS[n])
            if step < number:
                inputs["made", piece[0], step] = made[piece[0], step]
    outs = [("out", *piece) for piece in FINISHED[number]]
    for which in ("low", "high"):
        later = [
            piece
            for done in FINISHED[number + 1 :]
            for piece in done
            if piece[0] == which and any(block in blocks for block in members(piece))
        ]
        if later:
            outs.append(("made", which, number))
    shapes = [(piece_rows if name[0] == "out" else total, half) for name in outs]
    results = pl.pallas_call(
        functools.partial(expert_kernel, number, [*inputs, *outs]),
        in_specs=[SMEM] + [VMEM] * (4 + len(inputs)),
        out_shape=[jax.ShapeDtypeStruct(shape, jnp.bfloat16) for shape in shapes],
        scratch_shapes=[
            pltpu.VMEM((total, features), jnp.bfloat16),
            pltpu.VMEM((total, features), jnp.bfloat16),
            pltpu.VMEM((total, slots), jnp.float32),
        ],
        cost_estimate=pl.CostEstimate(
            flops=6 * total * units * features, bytes_accessed=4 * total * features, transcendentals=2 * total * units
        ),
        compiler_params=pltpu.CompilerParams(vmem_limit_bytes=28 << 20),
    )(place, weights, *projections, *inputs.values())
    results = dict(zip(outs, results))
    made.update({name[1:]: array for name, array in results.items() if name[0] == "made"})
    return {name[1:]: array for name, array in results.items() if name[0] == "out"}


def relay_kernel(along_y, place_ref, rows_ref, *refs):
    pieces, outs = refs[:SIDE], refs[SIDE:]
    y, x = place_ref[0], place_ref[1]
    tokens, slots = outs[0].shape[0], rows_ref.shape[2]
    step = tokens // 2
    token = lax.broadcasted_iota(jnp.int32, (step, slots), 0)
    lists = []
    for d in range(SIDE):
        lists.append(rows_ref[wrap(y + d) * SIDE + x if along_y else y * SIDE + wrap(x + d)])

    def work(i, carry):
        for t in range(SIDE):
            k = t if along_y else SIDE + t
            chosen = jnp.concatenate(
                [jnp.where(token + i * step == rows[k : k + 1, :], 1.0, 0.0).astype(jnp.bfloat16) for rows in lists], 1
            )
            rows = jnp.concatenate([piece[t * slots : (t + 1) * slots, :] for piece in pieces])
            total = jnp.dot(chosen, rows, preferred_element_type=jnp.float32)
            outs[t][pl.ds(pl.multiple_of(i * step, step), step), :] = total.astype(jnp.bfloat16)
        return carry

    lax.fori_loop(0, 2, work, 0)


def relay(along_y, place, rows, pieces, tokens):
    total, half = pieces[0].shape
    return pl.pallas_call(
        functools.partial(relay_kernel, along_y),
        in_specs=[SMEM] + [VMEM] * (1 + SIDE),
        out_shape=[jax.ShapeDtypeStruct((tokens, half), jnp.bfloat16)] * SIDE,
        cost_estimate=pl.CostEstimate(
            flops=2 * SIDE * total * tokens * half, bytes_accessed=4 << 20, transcendentals=0
        ),
        compiler_params=pltpu.CompilerParams(vmem_limit_bytes=12 << 20),
        name="relay_y" if along_y else "relay_x",
    )(place, rows, *pieces)


def add_kernel(*refs):
    out_ref = refs[-1]
    half = refs[0].shape[1]
    for n, parts in enumerate((refs[:SIDE], refs[SIDE : 2 * SIDE])):
        total = parts[0][...].astype(jnp.float32)
        for part in parts[1:]:
            total = total + part[...].astype(jnp.float32)
        out_ref[:, n * half : (n + 1) * half] = total.astype(jnp.bfloat16)


def add(lows, highs):
    tokens, half = lows[0].shape
    step = tokens // 4
    return pl.pallas_call(
        add_kernel,
        grid=(4,),
        in_specs=[pl.BlockSpec((step, half), lambda i: (i, 0))] * (2 * SIDE),
        out_specs=pl.BlockSpec((step, 2 * half), lambda i: (i, 0)),
        out_shape=jax.ShapeDtypeStruct((tokens, 2 * half), jnp.bfloat16),
        cost_estimate=pl.CostEstimate(flops=4_000_000, bytes_accessed=5 << 20, transcendentals=0),
        compiler_params=pltpu.CompilerParams(vmem_limit_bytes=12 << 20),
        name="add",
    )(*lows, *highs)


def over_plane(array, by_y, by_x):
    places = [(y, x) for y in range(SIDE) for x in range(SIDE)]
    return lax.ppermute(
        array, "ep", [(y * SIDE + x, (y + by_y) % SIDE * SIDE + (x + by_x) % SIDE) for y, x in places]
    )


def along_z(array, by, tp_count):
    chips = tp_count // 2
    return lax.ppermute(array, "tp", [(z * 2 + c, (z + by) % chips * 2 + c) for z in range(chips) for c in range(2)])


def other_core(array, tp_count):
    return lax.ppermute(array, "tp", [(j, j ^ 1) for j in range(tp_count)])


def layer(stream, norm_gain, gate_rows, up_rows, down_rows, chosen, affinity):
    ep_count = lax.axis_size("ep")
    tp_count = lax.axis_size("tp")
    block, _ = stream.shape
    slots = 4 * block // ep_count
    ep_index = lax.axis_index("ep").astype(jnp.int32)
    place = jnp.stack([ep_index // SIDE, ep_index % SIDE])
    bounds = (jnp.arange(ep_count, dtype=jnp.int32) * tp_count + lax.axis_index("tp")) * block
    low, high, own = prepare(stream, norm_gain, (gate_rows, up_rows, down_rows))
    lows = [low] + [over_plane(low, 0, t) for t in range(1, SIDE)]
    highs = [high] + [over_plane(high, t, 0) for t in range(1, SIDE)]
    ahead, behind = along_z(own, 1, tp_count), along_z(own, -1, tp_count)
    rows_there, weights = windows(bounds, chosen, affinity, block, slots)
    rows_here = lax.all_to_all(rows_there, "ep", split_axis=0, concat_axis=0, tiled=True)
    ahead2, behind2 = along_z(ahead, 1, tp_count), along_z(behind, -1, tp_count)
    picked_low = pick(True, place, rows_here, lows)
    arrived_low = [picked_low[0]] + [over_plane(picked_low[d], d, 0) for d in range(1, SIDE)]
    picked_high = pick(False, place, rows_here, highs)
    arrived_high = [picked_high[0]] + [over_plane(picked_high[d], 0, d) for d in range(1, SIDE)]
    cut = own.shape[1] // 2
    far = [
        along_z(ahead2[:, :cut], 2, tp_count),
        along_z(behind2[:, cut:], -2, tp_count),
        along_z(ahead2, 1, tp_count),
        along_z(behind2, -1, tp_count),
    ]
    early = stack([own, ahead, behind, ahead2, behind2])
    late = stack(far)
    pieces = [early, late, other_core(early, tp_count), other_core(late, tp_count)]
    projections = assemble(pieces)
    made, back = {}, {}
    for number in range(len(STEPS)):
        finished = expert(number, place, weights, projections, arrived_low, arrived_high, made)
        for (half, by), piece in finished.items():
            if by == 0:
                back[half, by] = piece
            elif half == "low":
                back[half, by] = over_plane(piece, -by, 0)
            else:
                back[half, by] = over_plane(piece, 0, -by)
    sums_low = relay(True, place, rows_here, [back["low", d] for d in range(SIDE)], block)
    sums_low = [sums_low[0]] + [over_plane(sums_low[t], 0, -t) for t in range(1, SIDE)]
    sums_high = relay(False, place, rows_here, [back["high", d] for d in range(SIDE)], block)
    sums_high = [sums_high[0]] + [over_plane(sums_high[t], -t, 0) for t in range(1, SIDE)]
    return add(sums_low, sums_high)


def solution(mesh):
    return jax.shard_map(
        layer,
        mesh=mesh,
        in_specs=(
            P(("ep", "tp"), None),
            P(),
            P("ep", "tp", None),
            P("ep", "tp", None),
            P("ep", "tp", None),
            P("ep", None),
            P("ep", None),
        ),
        out_specs=P(("ep", "tp"), None),
        check_vma=False,
    )
```

profile of v0, /device:TPU:4, one launch (start us, length us, event | category | flops | bytes accessed | tf_op | source)
XLA Modules:
  0.0 215.9 jit_solution(7493545153965309959)
XLA Ops:
  4.6 4.0 %collective-permute-start.1 = (bf16[3,64,1024]{2,1,0:T(8,128)(2,1)}, bf16[3,64,1024]{2,1,0:T(8,128)(2,1)S(1)}, u32[]{:S(2)}, u32[]{:S(2)}) collective-permute-start(bf16[3,64,1024]{2,1,0:T(8,128)(2,1)} %get-tuple-element.41.refs_0_), channel_id=1, source_target_pairs={{0,14},{1,15},{2,0},{3,1},{4,2},{5,3},{6,4},{7,5},{8,6},{9,7},{10,... | collective-permute-start | bytes 1179656 | tf_op jit(solution)/shard_map/ppermute | solution.py:359
  8.6 9.2 %collective-permute-done.refs_1_ = bf16[3,64,1024]{2,1,0:T(8,128)(2,1)S(1)} collective-permute-done((bf16[3,64,1024]{2,1,0:T(8,128)(2,1)}, bf16[3,64,1024]{2,1,0:T(8,128)(2,1)S(1)}, u32[]{:S(2)}, u32[]{:S(2)}) %collective-permute-start) | collective-permute-done | bytes 393248 | tf_op jit(solution)/shard_map/ppermute | solution.py:359
  17.8 3.2 %collective-permute-start.3 = (bf16[3,64,1024]{2,1,0:T(8,128)(2,1)S(1)}, bf16[3,64,1024]{2,1,0:T(8,128)(2,1)S(1)}, u32[]{:S(2)}, u32[]{:S(2)}) collective-permute-start(bf16[3,64,1024]{2,1,0:T(8,128)(2,1)S(1)} %collective-permute-done.1.refs_2_), channel_id=1, source_target_pairs={{0,14},{1,15},{2,0},{3,1},{4,2},{5,3},{6,4},{7,5},{8,6},{9,7},{10,... | collective-permute-start | bytes 1179656 | tf_op jit(solution)/shard_map/ppermute | solution.py:359
  21.1 8.2 %collective-permute-done.2.refs_3_ = bf16[3,64,1024]{2,1,0:T(8,128)(2,1)S(1)} collective-permute-done((bf16[3,64,1024]{2,1,0:T(8,128)(2,1)S(1)}, bf16[3,64,1024]{2,1,0:T(8,128)(2,1)S(1)}, u32[]{:S(2)}, u32[]{:S(2)}) %collective-permute-start.2) | collective-permute-done | bytes 393248 | tf_op jit(solution)/shard_map/ppermute | solution.py:359
  33.8 3.0 %collective-permute-start.6 = (bf16[3,64,1024]{2,1,0:T(8,128)(2,1)S(1)}, bf16[3,64,1024]{2,1,0:T(8,128)(2,1)S(1)}, u32[]{:S(2)}, u32[]{:S(2)}) collective-permute-start(bf16[3,64,1024]{2,1,0:T(8,128)(2,1)S(1)} %collective-permute-done.2.refs_3_), channel_id=1, source_target_pairs={{0,2},{1,3},{2,4},{3,5},{4,6},{5,7},{6,8},{7,9},{8,10},{9,11},{10,... | collective-permute-start | bytes 1179656 | tf_op jit(solution)/shard_map/ppermute | solution.py:359
  37.1 9.0 %collective-permute-done.4.refs_0_ = bf16[3,32,1024]{2,1,0:T(8,128)(2,1)S(1)} collective-permute-done((bf16[3,32,1024]{2,1,0:T(8,128)(2,1)S(1)}, bf16[3,32,1024]{2,1,0:T(8,128)(2,1)S(1)}, u32[]{:S(2)}, u32[]{:S(2)}) %collective-permute-start.4) | collective-permute-done | bytes 196640 | tf_op jit(solution)/shard_map/ppermute | solution.py:359
  46.1 9.9 %collective-permute-done.5.refs_1_ = bf16[3,32,1024]{2,1,0:T(8,128)(2,1)S(1)} collective-permute-done((bf16[3,32,1024]{2,1,0:T(8,128)(2,1)S(1)}, bf16[3,32,1024]{2,1,0:T(8,128)(2,1)S(1)}, u32[]{:S(2)}, u32[]{:S(2)}) %collective-permute-start.5) | collective-permute-done | bytes 196640 | tf_op jit(solution)/shard_map/ppermute | solution.py:359
  63.7 7.2 %all-to-all-start = ((s32[16,8,128]{2,1,0:T(8,128)}), s32[16,8,128]{2,1,0:T(8,128)S(1)}, u32[]{:S(2)}, u32[]{:S(2)}) async-start(s32[16,8,128]{2,1,0:T(8,128)} %get-tuple-element.39), calls=%async_computation | async-start | bytes 131072 | tf_op jit(solution)/shard_map/all_to_all | solution.py:379
  72.6 3.2 %collective-permute-start.16 = (bf16[512,512]{1,0:T(8,128)(2,1)}, bf16[512,512]{1,0:T(8,128)(2,1)}, u32[]{:S(2)}, u32[]{:S(2)}) collective-permute-start(bf16[512,512]{1,0:T(8,128)(2,1)} %get-tuple-element.49.refs_0_), channel_id=1, source_target_pairs={{0,128},{16,144},{32,160},{48,176},{64,192},{80,208},{96,224},{112... | collective-permute-start | bytes 1572872 | tf_op jit(solution)/shard_map/ppermute | solution.py:352
  75.8 7.5 %collective-permute-done.12.refs_3_ = bf16[512,512]{1,0:T(8,128)(2,1)} collective-permute-done((bf16[512,512]{1,0:T(8,128)(2,1)}, bf16[512,512]{1,0:T(8,128)(2,1)}, u32[]{:S(2)}, u32[]{:S(2)}) %collective-permute-start.12) | collective-permute-done | bytes 524320 | tf_op jit(solution)/shard_map/ppermute | solution.py:352
  83.3 3.0 %collective-permute-start.17 = (bf16[512,512]{1,0:T(8,128)(2,1)}, bf16[512,512]{1,0:T(8,128)(2,1)}, u32[]{:S(2)}, u32[]{:S(2)}) collective-permute-start(bf16[512,512]{1,0:T(8,128)(2,1)} %get-tuple-element.49.refs_0_), channel_id=1, source_target_pairs={{0,192},{16,208},{32,224},{48,240},{64,0},{80,16},{96,32},{112,48}... | collective-permute-start | bytes 1572872 | tf_op jit(solution)/shard_map/ppermute | solution.py:352
  87.4 2.9 %pick_y.1 = (bf16[512,512]{1,0:T(8,128)(2,1)S(1)}, bf16[512,512]{1,0:T(8,128)(2,1)S(1)}, bf16[512,512]{1,0:T(8,128)(2,1)S(1)}, bf16[512,512]{1,0:T(8,128)(2,1)S(1)}) custom-call(s32[2]{0:T(128)S(1)} %pad_add_fusion.place_ref, s32[16,8,128]{2,1,0:T(8,128)S(1)} %all-to-all-done.rows_ref, bf16[512,512]{1,0:T(8,128)(2,1)} %get-tuple-element.45.refs_0_, ...), custom_call_target="tpu_custom_call" | custom-call | flops 1073741824 | bytes 4194304 | tf_op jit(solution)/shard_map/pick_y/pallas_call | solution.py:127
  93.6 7.4 %collective-permute-done.17.refs_3_ = bf16[512,512]{1,0:T(8,128)(2,1)} collective-permute-done((bf16[512,512]{1,0:T(8,128)(2,1)}, bf16[512,512]{1,0:T(8,128)(2,1)}, u32[]{:S(2)}, u32[]{:S(2)}) %collective-permute-start.17) | collective-permute-done | bytes 524320 | tf_op jit(solution)/shard_map/ppermute | solution.py:352
  101.0 3.1 %pick_x.1 = (bf16[512,512]{1,0:T(8,128)(2,1)S(1)}, bf16[512,512]{1,0:T(8,128)(2,1)S(1)}, bf16[512,512]{1,0:T(8,128)(2,1)S(1)}, bf16[512,512]{1,0:T(8,128)(2,1)S(1)}) custom-call(s32[2]{0:T(128)S(1)} %pad_add_fusion.place_ref, s32[16,8,128]{2,1,0:T(8,128)S(1)} %all-to-all-done.rows_ref, bf16[512,512]{1,0:T(8,128)(2,1)} %get-tuple-element.49.refs_0_, ...), custom_call_target="tpu_custom_call" | custom-call | flops 1073741824 | bytes 4194304 | tf_op jit(solution)/shard_map/pick_x/pallas_call | solution.py:127
  110.9 10.1 %collective-permute-done.14.refs_3_.refs_2_ = bf16[512,512]{1,0:T(8,128)(2,1)S(1)} collective-permute-done((bf16[512,512]{1,0:T(8,128)(2,1)S(1)}, bf16[512,512]{1,0:T(8,128)(2,1)S(1)}, u32[]{:S(2)}, u32[]{:S(2)}) %collective-permute-start.14) | collective-permute-done | bytes 524320 | tf_op jit(solution)/shard_map/ppermute | solution.py:352
  121.0 8.2 %collective-permute-done.21.refs_6_ = bf16[512,512]{1,0:T(8,128)(2,1)S(1)} collective-permute-done((bf16[512,512]{1,0:T(8,128)(2,1)S(1)}, bf16[512,512]{1,0:T(8,128)(2,1)S(1)}, u32[]{:S(2)}, u32[]{:S(2)}) %collective-permute-start.21) | collective-permute-done | bytes 524320 | tf_op jit(solution)/shard_map/ppermute | solution.py:352
  129.2 8.0 %shard_map.75 = (bf16[512,512]{1,0:T(8,128)(2,1)S(1)}, bf16[512,512]{1,0:T(8,128)(2,1)S(1)}, bf16[1024,512]{1,0:T(8,128)(2,1)S(1)}, bf16[1024,512]{1,0:T(8,128)(2,1)S(1)}) custom-call(s32[2]{0:T(128)S(1)} %pad_add_fusion.place_ref, f32[16,128]{1,0:T(8,128)S(1)} %copy-done.3, bf16[1024,1024]{1,0:T(8,128)(2,1)S(1)} %get-tuple-element.42.gate_ref, ...), custom_call_target="tpu_custom_call" | custom-call | flops 6442450944 | bytes 4194304 | tf_op jit(solution)/shard_map/pallas_call | solution.py:268
  137.2 8.0 %shard_map.76 = (bf16[512,512]{1,0:T(8,128)(2,1)S(1)}, bf16[512,512]{1,0:T(8,128)(2,1)S(1)}, bf16[512,512]{1,0:T(8,128)(2,1)S(1)}, bf16[512,512]{1,0:T(8,128)(2,...) custom-call(s32[2]{0:T(128)S(1)} %pad_add_fusion.place_ref, f32[16,128]{1,0:T(8,128)S(1)} %copy-done.3, ...), custom_call_target="tpu_custom_call" | custom-call | flops 6442450944 | bytes 4194304 | tf_op jit(solution)/shard_map/pallas_call | solution.py:268
  148.3 3.3 %collective-permute-start.29 = (bf16[512,512]{1,0:T(8,128)(2,1)S(1)}, bf16[512,512]{1,0:T(8,128)(2,1)S(1)}, u32[]{:S(2)}, u32[]{:S(2)}) collective-permute-start(bf16[512,512]{1,0:T(8,128)(2,1)S(1)} %get-tuple-element.67), channel_id=1, source_target_pairs={{0,32},{16,48},{32,0},{48,16},{64,96},{80,112},{96,64},{112,80},{1... | collective-permute-start | bytes 1572872 | tf_op jit(solution)/shard_map/ppermute | solution.py:352
  151.6 16.6 %collective-permute-done.22.refs_1_ = bf16[512,512]{1,0:T(8,128)(2,1)S(1)} collective-permute-done((bf16[512,512]{1,0:T(8,128)(2,1)S(1)}, bf16[512,512]{1,0:T(8,128)(2,1)S(1)}, u32[]{:S(2)}, u32[]{:S(2)}) %collective-permute-start.22) | collective-permute-done | bytes 524320 | tf_op jit(solution)/shard_map/ppermute | solution.py:352
  168.2 3.7 %collective-permute-done.24.refs_3_ = bf16[512,512]{1,0:T(8,128)(2,1)S(1)} collective-permute-done((bf16[512,512]{1,0:T(8,128)(2,1)S(1)}, bf16[512,512]{1,0:T(8,128)(2,1)S(1)}, u32[]{:S(2)}, u32[]{:S(2)}) %collective-permute-start.24) | collective-permute-done | bytes 524320 | tf_op jit(solution)/shard_map/ppermute | solution.py:352
  179.3 18.7 %collective-permute-start.31 = (bf16[512,512]{1,0:T(8,128)(2,1)S(1)}, bf16[512,512]{1,0:T(8,128)(2,1)S(1)}, u32[]{:S(2)}, u32[]{:S(2)}) collective-permute-start(bf16[512,512]{1,0:T(8,128)(2,1)S(1)} %get-tuple-element.70), channel_id=1, source_target_pairs={{0,192},{16,208},{32,224},{48,240},{64,0},{80,16},{96,32},{112,48}... | collective-permute-start | bytes 1572872 | tf_op jit(solution)/shard_map/ppermute | solution.py:352
  200.2 10.2 %collective-permute-done.31.refs_5_ = bf16[512,512]{1,0:T(8,128)(2,1)S(1)} collective-permute-done((bf16[512,512]{1,0:T(8,128)(2,1)S(1)}, bf16[512,512]{1,0:T(8,128)(2,1)S(1)}, u32[]{:S(2)}, u32[]{:S(2)}) %collective-permute-start.31) | collective-permute-done | bytes 524320 | tf_op jit(solution)/shard_map/ppermute | solution.py:352
  210.4 3.7 %collective-permute-done.33.refs_7_ = bf16[512,512]{1,0:T(8,128)(2,1)S(1)} collective-permute-done((bf16[512,512]{1,0:T(8,128)(2,1)S(1)}, bf16[512,512]{1,0:T(8,128)(2,1)S(1)}, u32[]{:S(2)}, u32[]{:S(2)}) %collective-permute-start.33) | collective-permute-done | bytes 524320 | tf_op jit(solution)/shard_map/ppermute | solution.py:352
  (70 shorter events, 44.4 us)
Async XLA Ops:
  30.5 77.1 %collective-permute-start.8 = (bf16[3,320,1024]{2,1,0:T(8,128)(2,1)S(1)}, bf16[3,320,1024]{2,1,0:T(8,128)(2,1)}, u32[]{:S(2)}, u32[]{:S(2)}) collective-permute-start(bf16[3,320,1024]{2,1,0:T(8,128)(2,1)S(1)} %shard_map.73.refs_0_), channel_id=1, source_target_pairs={{0,1},{1,0},{2,3},{3,2},{4,5},{5,4},{6,7},{7,6},{8,9},{9,8},{10,11... | collective-permute-start | bytes 5898248 | tf_op jit(solution)/shard_map/ppermute | solution.py:363
  30.6 27.6 %collective-permute-start.10 = (bf16[512,512]{1,0:T(8,128)(2,1)}, bf16[512,512]{1,0:T(8,128)(2,1)S(1)}, u32[]{:S(2)}, u32[]{:S(2)}) collective-permute-start(bf16[512,512]{1,0:T(8,128)(2,1)} %get-tuple-element.45.refs_0_), channel_id=1, source_target_pairs={{0,16},{16,32},{32,48},{48,0},{64,80},{80,96},{96,112},{112,64},{1... | collective-permute-start | bytes 1572872 | tf_op jit(solution)/shard_map/ppermute | solution.py:352
  33.8 22.1 %collective-permute-start.6 = (bf16[3,64,1024]{2,1,0:T(8,128)(2,1)S(1)}, bf16[3,64,1024]{2,1,0:T(8,128)(2,1)S(1)}, u32[]{:S(2)}, u32[]{:S(2)}) collective-permute-start(bf16[3,64,1024]{2,1,0:T(8,128)(2,1)S(1)} %collective-permute-done.2.refs_3_), channel_id=1, source_target_pairs={{0,2},{1,3},{2,4},{3,5},{4,6},{5,7},{6,8},{7,9},{8,10},{9,11},{10,... | collective-permute-start | bytes 1179656 | tf_op jit(solution)/shard_map/ppermute | solution.py:359
  36.8 19.2 %collective-permute-start.7 = (bf16[3,64,1024]{2,1,0:T(8,128)(2,1)S(1)}, bf16[3,64,1024]{2,1,0:T(8,128)(2,1)S(1)}, u32[]{:S(2)}, u32[]{:S(2)}) collective-permute-start(bf16[3,64,1024]{2,1,0:T(8,128)(2,1)S(1)} %collective-permute-done.3.refs_4_), channel_id=1, source_target_pairs={{0,14},{1,15},{2,0},{3,1},{4,2},{5,3},{6,4},{7,5},{8,6},{9,7},{10,... | collective-permute-start | bytes 1179656 | tf_op jit(solution)/shard_map/ppermute | solution.py:359
  56.0 50.1 %collective-permute-start.9 = (bf16[3,192,1024]{2,1,0:T(8,128)(2,1)S(1)}, bf16[3,192,1024]{2,1,0:T(8,128)(2,1)}, u32[]{:S(2)}, u32[]{:S(2)}) collective-permute-start(bf16[3,192,1024]{2,1,0:T(8,128)(2,1)S(1)} %shard_map.74.refs_1_), channel_id=1, source_target_pairs={{0,1},{1,0},{2,3},{3,2},{4,5},{5,4},{6,7},{7,6},{8,9},{9,8},{10,11... | collective-permute-start | bytes 3538952 | tf_op jit(solution)/shard_map/ppermute | solution.py:363
  56.2 16.5 %collective-permute-start.11 = (bf16[512,512]{1,0:T(8,128)(2,1)}, bf16[512,512]{1,0:T(8,128)(2,1)}, u32[]{:S(2)}, u32[]{:S(2)}) collective-permute-start(bf16[512,512]{1,0:T(8,128)(2,1)} %get-tuple-element.45.refs_0_), channel_id=1, source_target_pairs={{0,32},{16,48},{32,0},{48,16},{64,96},{80,112},{96,64},{112,80},{1... | collective-permute-start | bytes 1572872 | tf_op jit(solution)/shard_map/ppermute | solution.py:352
  57.0 26.3 %collective-permute-start.12 = (bf16[512,512]{1,0:T(8,128)(2,1)}, bf16[512,512]{1,0:T(8,128)(2,1)}, u32[]{:S(2)}, u32[]{:S(2)}) collective-permute-start(bf16[512,512]{1,0:T(8,128)(2,1)} %get-tuple-element.45.refs_0_), channel_id=1, source_target_pairs={{0,48},{16,0},{32,16},{48,32},{64,112},{80,64},{96,80},{112,96},{1... | collective-permute-start | bytes 1572872 | tf_op jit(solution)/shard_map/ppermute | solution.py:352
  59.0 31.3 %collective-permute-start.15 = (bf16[512,512]{1,0:T(8,128)(2,1)}, bf16[512,512]{1,0:T(8,128)(2,1)}, u32[]{:S(2)}, u32[]{:S(2)}) collective-permute-start(bf16[512,512]{1,0:T(8,128)(2,1)} %get-tuple-element.49.refs_0_), channel_id=1, source_target_pairs={{0,64},{16,80},{32,96},{48,112},{64,128},{80,144},{96,160},{112,17... | collective-permute-start | bytes 1572872 | tf_op jit(solution)/shard_map/ppermute | solution.py:352
  63.7 22.6 %all-to-all-start = ((s32[16,8,128]{2,1,0:T(8,128)}), s32[16,8,128]{2,1,0:T(8,128)S(1)}, u32[]{:S(2)}, u32[]{:S(2)}) async-start(s32[16,8,128]{2,1,0:T(8,128)} %get-tuple-element.39), calls=%async_computation | async-start | bytes 131072 | tf_op jit(solution)/shard_map/all_to_all | solution.py:379
  72.6 18.3 %collective-permute-start.16 = (bf16[512,512]{1,0:T(8,128)(2,1)}, bf16[512,512]{1,0:T(8,128)(2,1)}, u32[]{:S(2)}, u32[]{:S(2)}) collective-permute-start(bf16[512,512]{1,0:T(8,128)(2,1)} %get-tuple-element.49.refs_0_), channel_id=1, source_target_pairs={{0,128},{16,144},{32,160},{48,176},{64,192},{80,208},{96,224},{112... | collective-permute-start | bytes 1572872 | tf_op jit(solution)/shard_map/ppermute | solution.py:352
  83.3 17.7 %collective-permute-start.17 = (bf16[512,512]{1,0:T(8,128)(2,1)}, bf16[512,512]{1,0:T(8,128)(2,1)}, u32[]{:S(2)}, u32[]{:S(2)}) collective-permute-start(bf16[512,512]{1,0:T(8,128)(2,1)} %get-tuple-element.49.refs_0_), channel_id=1, source_target_pairs={{0,192},{16,208},{32,224},{48,240},{64,0},{80,16},{96,32},{112,48}... | collective-permute-start | bytes 1572872 | tf_op jit(solution)/shard_map/ppermute | solution.py:352
  90.9 30.1 %collective-permute-start.14 = (bf16[512,512]{1,0:T(8,128)(2,1)S(1)}, bf16[512,512]{1,0:T(8,128)(2,1)S(1)}, u32[]{:S(2)}, u32[]{:S(2)}) collective-permute-start(bf16[512,512]{1,0:T(8,128)(2,1)S(1)} %get-tuple-element.48), channel_id=1, source_target_pairs={{0,192},{16,208},{32,224},{48,240},{64,0},{80,16},{96,32},{112,48}... | collective-permute-start | bytes 1572872 | tf_op jit(solution)/shard_map/ppermute | solution.py:352
  104.1 16.9 %collective-permute-start.18 = (bf16[512,512]{1,0:T(8,128)(2,1)S(1)}, bf16[512,512]{1,0:T(8,128)(2,1)S(1)}, u32[]{:S(2)}, u32[]{:S(2)}) collective-permute-start(bf16[512,512]{1,0:T(8,128)(2,1)S(1)} %get-tuple-element.51), channel_id=1, source_target_pairs={{0,48},{16,0},{32,16},{48,32},{64,112},{80,64},{96,80},{112,96},{1... | collective-permute-start | bytes 1572872 | tf_op jit(solution)/shard_map/ppermute | solution.py:352
  107.5 21.7 %collective-permute-start.21 = (bf16[512,512]{1,0:T(8,128)(2,1)S(1)}, bf16[512,512]{1,0:T(8,128)(2,1)S(1)}, u32[]{:S(2)}, u32[]{:S(2)}) collective-permute-start(bf16[512,512]{1,0:T(8,128)(2,1)S(1)} %get-tuple-element.54), channel_id=1, source_target_pairs={{0,32},{16,48},{32,0},{48,16},{64,96},{80,112},{96,64},{112,80},{1... | collective-permute-start | bytes 1572872 | tf_op jit(solution)/shard_map/ppermute | solution.py:352
  145.3 22.9 %collective-permute-start.22 = (bf16[512,512]{1,0:T(8,128)(2,1)S(1)}, bf16[512,512]{1,0:T(8,128)(2,1)S(1)}, u32[]{:S(2)}, u32[]{:S(2)}) collective-permute-start(bf16[512,512]{1,0:T(8,128)(2,1)S(1)} %get-tuple-element.58), channel_id=1, source_target_pairs={{0,192},{16,208},{32,224},{48,240},{64,0},{80,16},{96,32},{112,48}... | collective-permute-start | bytes 1572872 | tf_op jit(solution)/shard_map/ppermute | solution.py:352
  147.3 20.8 %collective-permute-start.23 = (bf16[512,512]{1,0:T(8,128)(2,1)S(1)}, bf16[512,512]{1,0:T(8,128)(2,1)S(1)}, u32[]{:S(2)}, u32[]{:S(2)}) collective-permute-start(bf16[512,512]{1,0:T(8,128)(2,1)S(1)} %get-tuple-element.59), channel_id=1, source_target_pairs={{0,128},{16,144},{32,160},{48,176},{64,192},{80,208},{96,224},{112... | collective-permute-start | bytes 1572872 | tf_op jit(solution)/shard_map/ppermute | solution.py:352
  147.6 24.2 %collective-permute-start.24 = (bf16[512,512]{1,0:T(8,128)(2,1)S(1)}, bf16[512,512]{1,0:T(8,128)(2,1)S(1)}, u32[]{:S(2)}, u32[]{:S(2)}) collective-permute-start(bf16[512,512]{1,0:T(8,128)(2,1)S(1)} %get-tuple-element.60), channel_id=1, source_target_pairs={{0,64},{16,80},{32,96},{48,112},{64,128},{80,144},{96,160},{112,17... | collective-permute-start | bytes 1572872 | tf_op jit(solution)/shard_map/ppermute | solution.py:352
  148.3 26.8 %collective-permute-start.28 = (bf16[512,512]{1,0:T(8,128)(2,1)S(1)}, bf16[512,512]{1,0:T(8,128)(2,1)S(1)}, u32[]{:S(2)}, u32[]{:S(2)}) collective-permute-start(bf16[512,512]{1,0:T(8,128)(2,1)S(1)} %get-tuple-element.66), channel_id=1, source_target_pairs={{0,48},{16,0},{32,16},{48,32},{64,112},{80,64},{96,80},{112,96},{1... | collective-permute-start | bytes 1572872 | tf_op jit(solution)/shard_map/ppermute | solution.py:352
  148.3 29.0 %collective-permute-start.29 = (bf16[512,512]{1,0:T(8,128)(2,1)S(1)}, bf16[512,512]{1,0:T(8,128)(2,1)S(1)}, u32[]{:S(2)}, u32[]{:S(2)}) collective-permute-start(bf16[512,512]{1,0:T(8,128)(2,1)S(1)} %get-tuple-element.67), channel_id=1, source_target_pairs={{0,32},{16,48},{32,0},{48,16},{64,96},{80,112},{96,64},{112,80},{1... | collective-permute-start | bytes 1572872 | tf_op jit(solution)/shard_map/ppermute | solution.py:352
  173.8 24.2 %collective-permute-start.25 = (bf16[512,512]{1,0:T(8,128)(2,1)S(1)}, bf16[512,512]{1,0:T(8,128)(2,1)S(1)}, u32[]{:S(2)}, u32[]{:S(2)}) collective-permute-start(bf16[512,512]{1,0:T(8,128)(2,1)S(1)} %get-tuple-element.62), channel_id=1, source_target_pairs={{0,48},{16,0},{32,16},{48,32},{64,112},{80,64},{96,80},{112,96},{1... | collective-permute-start | bytes 1572872 | tf_op jit(solution)/shard_map/ppermute | solution.py:352
  173.9 25.1 %collective-permute-start.26 = (bf16[512,512]{1,0:T(8,128)(2,1)S(1)}, bf16[512,512]{1,0:T(8,128)(2,1)S(1)}, u32[]{:S(2)}, u32[]{:S(2)}) collective-permute-start(bf16[512,512]{1,0:T(8,128)(2,1)S(1)} %get-tuple-element.63), channel_id=1, source_target_pairs={{0,32},{16,48},{32,0},{48,16},{64,96},{80,112},{96,64},{112,80},{1... | collective-permute-start | bytes 1572872 | tf_op jit(solution)/shard_map/ppermute | solution.py:352
  175.1 25.1 %collective-permute-start.27 = (bf16[512,512]{1,0:T(8,128)(2,1)S(1)}, bf16[512,512]{1,0:T(8,128)(2,1)S(1)}, u32[]{:S(2)}, u32[]{:S(2)}) collective-permute-start(bf16[512,512]{1,0:T(8,128)(2,1)S(1)} %get-tuple-element.64), channel_id=1, source_target_pairs={{0,16},{16,32},{32,48},{48,0},{64,80},{80,96},{96,112},{112,64},{1... | collective-permute-start | bytes 1572872 | tf_op jit(solution)/shard_map/ppermute | solution.py:352
  179.3 31.0 %collective-permute-start.31 = (bf16[512,512]{1,0:T(8,128)(2,1)S(1)}, bf16[512,512]{1,0:T(8,128)(2,1)S(1)}, u32[]{:S(2)}, u32[]{:S(2)}) collective-permute-start(bf16[512,512]{1,0:T(8,128)(2,1)S(1)} %get-tuple-element.70), channel_id=1, source_target_pairs={{0,192},{16,208},{32,224},{48,240},{64,0},{80,16},{96,32},{112,48}... | collective-permute-start | bytes 1572872 | tf_op jit(solution)/shard_map/ppermute | solution.py:352
  198.1 16.0 %collective-permute-start.33 = (bf16[512,512]{1,0:T(8,128)(2,1)S(1)}, bf16[512,512]{1,0:T(8,128)(2,1)S(1)}, u32[]{:S(2)}, u32[]{:S(2)}) collective-permute-start(bf16[512,512]{1,0:T(8,128)(2,1)S(1)} %get-tuple-element.72), channel_id=1, source_target_pairs={{0,64},{16,80},{32,96},{48,112},{64,128},{80,144},{96,160},{112,17... | collective-permute-start | bytes 1572872 | tf_op jit(solution)/shard_map/ppermute | solution.py:352
  (15 other events, 167.2 us)
where the time goes:
time: 216 us
  waiting for transfers between devices  107 us (50%)
  starting transfers between devices  70.3 us (33%)
  Pallas kernels  35.3 us (16%)
  local copies, waits for them, and re-layouts  2.89 us (1%)
    ppermute x24, waiting for transfers between devices, over_plane(): lax.ppermute(array, 'ep', [(y * SIDE + x, (y + by_y) % SIDE * SIDE + (x +...  70.2 us
    ppermute x24, starting transfers between devices, over_plane(): lax.ppermute(array, 'ep', [(y * SIDE + x, (y + by_y) % SIDE * SIDE + (x +...  48.4 us
    ppermute x8, waiting for transfers between devices, along_z(): lax.ppermute(array, 'tp', [(z * 2 + c, (z + by) % chips * 2 + c) for z in...  36.4 us
    pallas_call x2, Pallas kernels, expert(): pl.pallas_call(functools.partial(expert_kernel, number, [*inputs, *outs])...  16 us
    ppermute x8, starting transfers between devices, along_z(): lax.ppermute(array, 'tp', [(z * 2 + c, (z + by) % chips * 2 + c) for z in...  14.5 us
    all_to_all x1, starting transfers between devices, layer(): lax.all_to_all(rows_there, 'ep', split_axis=0, concat_axis=0, tiled=True)  7.24 us
    pallas_call x2, Pallas kernels, pick(): pl.pallas_call(functools.partial(pick_kernel, along_y), in_specs=[SMEM] +...  5.96 us
  transfers between devices with their start and end apart: 35, of which 15 were waited for; matrix products, arithmetic and copies ran while one was open for 0% of the time, Pallas kernels for 7%

commit v1 on v0

--- a/solution.py
+++ b/solution.py
@@ -21,8 +21,9 @@
     listed = list_ref[...]
     lines = listed.shape[0]
     lane = lax.broadcasted_iota(jnp.int32, (1, slots), 1)
-    for j in range(weights_ref.shape[0]):
-        y, x = divmod(j, SIDE)
+
+    def cut(j, carry):
+        y, x = j // SIDE, lax.rem(j, SIDE)
         bound = bounds_ref[j]
         start = jnp.sum((listed < bound).astype(jnp.int32))
         line, shift = start // slots, start % slots
@@ -38,9 +39,12 @@
         rows = window(list_ref) - bound
         rows = jnp.where((rows >= 0) & (rows < block), rows, -1)
         for t in range(SIDE):
-            rows_ref[y * SIDE + (x + t) % SIDE, t : t + 1, :] = rows
-            rows_ref[(y + t) % SIDE * SIDE + x, SIDE + t : SIDE + t + 1, :] = rows
-        weights_ref[j : j + 1, :] = window(affinity_ref)
+            rows_ref[y * SIDE + wrap(x + t - SIDE), t : t + 1, :] = rows
+            rows_ref[wrap(y + t - SIDE) * SIDE + x, SIDE + t : SIDE + t + 1, :] = rows
+        weights_ref[pl.ds(j, 1), :] = window(affinity_ref)
+        return carry
+
+    lax.fori_loop(0, weights_ref.shape[0], cut, 0, unroll=4)
 
 
 def windows(bounds, listed, affinity, block, slots):
@@ -102,23 +106,34 @@
     )(stream, norm_gain.reshape(1, features), *parts)
 
 
-def pick_kernel(along_y, place_ref, rows_ref, *refs):
-    sources, outs = refs[:SIDE], refs[SIDE:]
+def pick_kernel(along_y, place_ref, rows_ref, own_ref, after_ref, top_ref, bottom_ref, before_ref, *refs):
+    outs = refs[:SIDE]
+    across_ref, chosen_ref = refs[SIDE:]
     y, x = place_ref[0], place_ref[1]
-    tokens, slots = sources[0].shape[0], rows_ref.shape[2]
+    tokens, half = own_ref.shape
+    slots = rows_ref.shape[2]
+    across_ref[: tokens // 2, :] = top_ref[...]
+    across_ref[tokens // 2 :, :] = bottom_ref[...]
     token = lax.broadcasted_iota(jnp.int32, (slots, tokens), 1).astype(jnp.float32)
-    columns = []
     for d in range(SIDE):
         e = wrap(y + d) * SIDE + x if along_y else y * SIDE + wrap(x + d)
-        columns.append(rows_ref[e].astype(jnp.float32).T)
-    for t in range(SIDE):
-        k = t if along_y else SIDE + t
-        chosen = jnp.concatenate(
-            [jnp.where(column[:, k : k + 1] == token, 1.0, 0.0).astype(jnp.bfloat16) for column in columns]
-        )
-        rows = jnp.dot(chosen, sources[t][...], preferred_element_type=jnp.float32).astype(jnp.bfloat16)
-        for d in range(SIDE):
-            outs[d][t * slots : (t + 1) * slots, :] = rows[d * slots : (d + 1) * slots, :]
+        column = rows_ref[e].astype(jnp.float32).T
+        for t in range(SIDE):
+            k = t if along_y else SIDE + t
+            chosen_ref[t, d * slots : (d + 1) * slots, :] = jnp.where(column[:, k : k + 1] == token, 1.0, 0.0).astype(
+                jnp.bfloat16
+            )
+    step = half // 2
+
+    def work(i, carry):
+        at = pl.ds(pl.multiple_of(i * step, step), step)
+        for t, source in enumerate((own_ref, after_ref, across_ref, before_ref)):
+            rows = jnp.dot(chosen_ref[t], source[:, at], preferred_element_type=jnp.float32).astype(jnp.bfloat16)
+            for d in range(SIDE):
+                outs[d][t * slots : (t + 1) * slots, at] = rows[d * slots : (d + 1) * slots, :]
+        return carry
+
+    lax.fori_loop(0, 2, work, 0)
 
 
 def pick(along_y, place, rows, sources):
@@ -126,12 +141,16 @@
     slots = rows.shape[2]
     return pl.pallas_call(
         functools.partial(pick_kernel, along_y),
-        in_specs=[SMEM] + [VMEM] * (1 + SIDE),
+        in_specs=[SMEM] + [VMEM] * 6,
         out_shape=[jax.ShapeDtypeStruct((SIDE * slots, half), jnp.bfloat16)] * SIDE,
+        scratch_shapes=[
+            pltpu.VMEM((tokens, half), jnp.bfloat16),
+            pltpu.VMEM((SIDE, SIDE * slots, tokens), jnp.bfloat16),
+        ],
         cost_estimate=pl.CostEstimate(
             flops=2 * SIDE * SIDE * slots * tokens * half, bytes_accessed=4 << 20, transcendentals=0
         ),
-        compiler_params=pltpu.CompilerParams(vmem_limit_bytes=12 << 20),
+        compiler_params=pltpu.CompilerParams(vmem_limit_bytes=14 << 20),
         name="pick_y" if along_y else "pick_x",
     )(place, rows, *sources)
 
@@ -158,11 +177,18 @@
 
 def assemble_kernel(*refs):
     pieces, outs = refs[:-3], refs[-3:]
+    step = 64
     at = 0
     for piece in pieces:
         width = piece.shape[1]
         for j, out in enumerate(outs):
-            out[at : at + width, :] = piece[j]
+
+            def move(i, carry, piece=piece, out=out, j=j, at=at):
+                rows = pl.multiple_of(i * step, step)
+                out[pl.ds(at + rows, step), :] = piece[j, pl.ds(rows, step), :]
+                return carry
+
+            lax.fori_loop(0, width // step, move, 0)
         at += width
 
 
@@ -372,11 +398,14 @@
     place = jnp.stack([ep_index // SIDE, ep_index % SIDE])
     bounds = (jnp.arange(ep_count, dtype=jnp.int32) * tp_count + lax.axis_index("tp")) * block
     low, high, own = prepare(stream, norm_gain, (gate_rows, up_rows, down_rows))
-    lows = [low] + [over_plane(low, 0, t) for t in range(1, SIDE)]
-    highs = [high] + [over_plane(high, t, 0) for t in range(1, SIDE)]
+    left, right = over_plane(low, 0, 1), over_plane(low, 0, -1)
+    down, up = over_plane(high, 1, 0), over_plane(high, -1, 0)
     ahead, behind = along_z(own, 1, tp_count), along_z(own, -1, tp_count)
     rows_there, weights = windows(bounds, chosen, affinity, block, slots)
     rows_here = lax.all_to_all(rows_there, "ep", split_axis=0, concat_axis=0, tiled=True)
+    mid = block // 2
+    lows = [low, left, over_plane(left[:mid], 0, 1), over_plane(right[mid:], 0, -1), right]
+    highs = [high, down, over_plane(down[:mid], 1, 0), over_plane(up[mid:], -1, 0), up]
     ahead2, behind2 = along_z(ahead, 1, tp_count), along_z(behind, -1, tp_count)
     picked_low = pick(True, place, rows_here, lows)
     arrived_low = [picked_low[0]] + [over_plane(picked_low[d], d, 0) for d in range(1, SIDE)]

time: 216 us -> 218 us (level)
  the two profiles are of different devices: /device:TPU:4 before, /device:TPU:8 now
where the time goes in v1:
time: 218 us
  waiting for transfers between devices  125 us (57%)
  starting transfers between devices  47.8 us (22%)
  Pallas kernels  35.9 us (16%)
  local copies, waits for them, and re-layouts  8.42 us (4%)
    ppermute x26, waiting for transfers between devices, over_plane(): lax.ppermute(array, 'ep', [(y * SIDE + x, (y + by_y) % SIDE * SIDE + (x +...  86.8 us
    ppermute x8, waiting for transfers between devices, along_z(): lax.ppermute(array, 'tp', [(z * 2 + c, (z + by) % chips * 2 + c) for z in...  31.6 us
    ppermute x26, starting transfers between devices, over_plane(): lax.ppermute(array, 'ep', [(y * SIDE + x, (y + by_y) % SIDE * SIDE + (x +...  27.1 us
    pallas_call x2, Pallas kernels, expert(): pl.pallas_call(functools.partial(expert_kernel, number, [*inputs, *outs])...  16 us
    ppermute x8, starting transfers between devices, along_z(): lax.ppermute(array, 'tp', [(z * 2 + c, (z + by) % chips * 2 + c) for z in...  14.8 us
    pallas_call x2, Pallas kernels, pick(): pl.pallas_call(functools.partial(pick_kernel, along_y), in_specs=[SMEM] +...  6.32 us
    all_to_all x1, waiting for transfers between devices, layer(): lax.all_to_all(rows_there, 'ep', split_axis=0, concat_axis=0, tiled=True)  6.19 us
    all_to_all x1, starting transfers between devices, layer(): lax.all_to_all(rows_there, 'ep', split_axis=0, concat_axis=0, tiled=True)  5.78 us
  transfers between devices with their start and end apart: 37, of which 18 were waited for; matrix products, arithmetic and copies ran while one was open for 2% of the time, Pallas kernels for 7%

profile of v1, /device:TPU:8, one launch (start us, length us, event | category | flops | bytes accessed | tf_op | source)
XLA Modules:
  0.0 217.5 jit_solution(16500169948887157328)
XLA Ops:
  4.6 4.0 %collective-permute-start.1 = (bf16[3,64,1024]{2,1,0:T(8,128)(2,1)}, bf16[3,64,1024]{2,1,0:T(8,128)(2,1)S(1)}, u32[]{:S(2)}, u32[]{:S(2)}) collective-permute-start(bf16[3,64,1024]{2,1,0:T(8,128)(2,1)} %get-tuple-element.41.refs_0_), channel_id=1, source_target_pairs={{0,14},{1,15},{2,0},{3,1},{4,2},{5,3},{6,4},{7,5},{8,6},{9,7},{10,... | collective-permute-start | bytes 1179656 | tf_op jit(solution)/shard_map/ppermute | solution.py:385
  8.6 9.2 %collective-permute-done.refs_1_ = bf16[3,64,1024]{2,1,0:T(8,128)(2,1)S(1)} collective-permute-done((bf16[3,64,1024]{2,1,0:T(8,128)(2,1)}, bf16[3,64,1024]{2,1,0:T(8,128)(2,1)S(1)}, u32[]{:S(2)}, u32[]{:S(2)}) %collective-permute-start) | collective-permute-done | bytes 393248 | tf_op jit(solution)/shard_map/ppermute | solution.py:385
  17.9 3.2 %collective-permute-start.3 = (bf16[3,64,1024]{2,1,0:T(8,128)(2,1)S(1)}, bf16[3,64,1024]{2,1,0:T(8,128)(2,1)S(1)}, u32[]{:S(2)}, u32[]{:S(2)}) collective-permute-start(bf16[3,64,1024]{2,1,0:T(8,128)(2,1)S(1)} %collective-permute-done.1.refs_2_), channel_id=1, source_target_pairs={{0,14},{1,15},{2,0},{3,1},{4,2},{5,3},{6,4},{7,5},{8,6},{9,7},{10,... | collective-permute-start | bytes 1179656 | tf_op jit(solution)/shard_map/ppermute | solution.py:385
  21.1 8.2 %collective-permute-done.2.refs_3_ = bf16[3,64,1024]{2,1,0:T(8,128)(2,1)S(1)} collective-permute-done((bf16[3,64,1024]{2,1,0:T(8,128)(2,1)S(1)}, bf16[3,64,1024]{2,1,0:T(8,128)(2,1)S(1)}, u32[]{:S(2)}, u32[]{:S(2)}) %collective-permute-start.2) | collective-permute-done | bytes 393248 | tf_op jit(solution)/shard_map/ppermute | solution.py:385
  37.4 7.4 %collective-permute-done.4.refs_0_ = bf16[3,32,1024]{2,1,0:T(8,128)(2,1)S(1)} collective-permute-done((bf16[3,32,1024]{2,1,0:T(8,128)(2,1)S(1)}, bf16[3,32,1024]{2,1,0:T(8,128)(2,1)S(1)}, u32[]{:S(2)}, u32[]{:S(2)}) %collective-permute-start.4) | collective-permute-done | bytes 196640 | tf_op jit(solution)/shard_map/ppermute | solution.py:385
  45.1 2.8 %collective-permute-start.12 = (bf16[512,512]{1,0:T(8,128)(2,1)S(1)}, bf16[512,512]{1,0:T(8,128)(2,1)S(1)}, u32[]{:S(2)}, u32[]{:S(2)}) collective-permute-start(bf16[512,512]{1,0:T(8,128)(2,1)S(1)} %copy-done.5), channel_id=1, source_target_pairs={{0,48},{16,0},{32,16},{48,32},{64,112},{80,64},{96,80},{112,96},{1... | collective-permute-start | bytes 1572872 | tf_op jit(solution)/shard_map/ppermute | solution.py:378
  47.8 4.0 %collective-permute-done.6.refs_2_ = bf16[3,64,1024]{2,1,0:T(8,128)(2,1)S(1)} collective-permute-done((bf16[3,64,1024]{2,1,0:T(8,128)(2,1)S(1)}, bf16[3,64,1024]{2,1,0:T(8,128)(2,1)S(1)}, u32[]{:S(2)}, u32[]{:S(2)}) %collective-permute-start.6) | collective-permute-done | bytes 393248 | tf_op jit(solution)/shard_map/ppermute | solution.py:385
  51.8 2.7 %collective-permute-done.7.refs_3_ = bf16[3,64,1024]{2,1,0:T(8,128)(2,1)S(1)} collective-permute-done((bf16[3,64,1024]{2,1,0:T(8,128)(2,1)S(1)}, bf16[3,64,1024]{2,1,0:T(8,128)(2,1)S(1)}, u32[]{:S(2)}, u32[]{:S(2)}) %collective-permute-start.7) | collective-permute-done | bytes 393248 | tf_op jit(solution)/shard_map/ppermute | solution.py:385
  60.9 4.5 %collective-permute-done.11.top_ref = bf16[256,512]{1,0:T(8,128)(2,1)S(1)} collective-permute-done((bf16[256,512]{1,0:T(8,128)(2,1)S(1)}, bf16[256,512]{1,0:T(8,128)(2,1)S(1)}, u32[]{:S(2)}, u32[]{:S(2)}) %collective-permute-start.11) | collective-permute-done | bytes 262176 | tf_op jit(solution)/shard_map/ppermute | solution.py:378
  69.5 5.8 %all-to-all-start = ((s32[16,8,128]{2,1,0:T(8,128)}), s32[16,8,128]{2,1,0:T(8,128)S(1)}, u32[]{:S(2)}, u32[]{:S(2)}) async-start(s32[16,8,128]{2,1,0:T(8,128)} %get-tuple-element.39), calls=%async_computation | async-start | bytes 131072 | tf_op jit(solution)/shard_map/all_to_all | solution.py:405
  75.3 6.2 %all-to-all-done.rows_ref = s32[16,8,128]{2,1,0:T(8,128)S(1)} async-done(((s32[16,8,128]{2,1,0:T(8,128)}), s32[16,8,128]{2,1,0:T(8,128)S(1)}, u32[]{:S(2)}, u32[]{:S(2)}) %all-to-all-start) | async-done | bytes 65568 | tf_op jit(solution)/shard_map/all_to_all | solution.py:405
  84.7 3.0 %pick_y.1 = (bf16[512,512]{1,0:T(8,128)(2,1)S(1)}, bf16[512,512]{1,0:T(8,128)(2,1)S(1)}, bf16[512,512]{1,0:T(8,128)(2,1)S(1)}, bf16[512,512]{1,0:T(8,128)(2,1)S(1)}) custom-call(s32[2]{0:T(128)S(1)} %pad_add_fusion.place_ref, s32[16,8,128]{2,1,0:T(8,128)S(1)} %all-to-all-done.rows_ref, bf16[512,512]{1,0:T(8,128)(2,1)S(1)} %copy-done.6, ...), custom_call_target="tpu_custom_call" | custom-call | flops 1073741824 | bytes 4194304 | tf_op jit(solution)/shard_map/pick_y/pallas_call | solution.py:142
  92.4 12.7 %collective-permute-done.17.top_ref = bf16[256,512]{1,0:T(8,128)(2,1)S(1)} collective-permute-done((bf16[256,512]{1,0:T(8,128)(2,1)S(1)}, bf16[256,512]{1,0:T(8,128)(2,1)S(1)}, u32[]{:S(2)}, u32[]{:S(2)}) %collective-permute-start.17) | collective-permute-done | bytes 262176 | tf_op jit(solution)/shard_map/ppermute | solution.py:378
  105.2 2.7 %collective-permute-start.15 = (bf16[512,512]{1,0:T(8,128)(2,1)S(1)}, bf16[512,512]{1,0:T(8,128)(2,1)S(1)}, u32[]{:S(2)}, u32[]{:S(2)}) collective-permute-start(bf16[512,512]{1,0:T(8,128)(2,1)S(1)} %get-tuple-element.48), channel_id=1, source_target_pairs={{0,192},{16,208},{32,224},{48,240},{64,0},{80,16},{96,32},{112,48}... | collective-permute-start | bytes 1572872 | tf_op jit(solution)/shard_map/ppermute | solution.py:378
  107.9 3.4 %pick_x.1 = (bf16[512,512]{1,0:T(8,128)(2,1)S(1)}, bf16[512,512]{1,0:T(8,128)(2,1)S(1)}, bf16[512,512]{1,0:T(8,128)(2,1)S(1)}, bf16[512,512]{1,0:T(8,128)(2,1)S(1)}) custom-call(s32[2]{0:T(128)S(1)} %pad_add_fusion.place_ref, s32[16,8,128]{2,1,0:T(8,128)S(1)} %all-to-all-done.rows_ref, bf16[512,512]{1,0:T(8,128)(2,1)} %get-tuple-element.49.own_ref, ...), custom_call_target="tpu_custom_call" | custom-call | flops 1073741824 | bytes 4194304 | tf_op jit(solution)/shard_map/pick_x/pallas_call | solution.py:142
  117.4 2.8 %collective-permute-done.15.refs_3_.refs_2_ = bf16[512,512]{1,0:T(8,128)(2,1)S(1)} collective-permute-done((bf16[512,512]{1,0:T(8,128)(2,1)S(1)}, bf16[512,512]{1,0:T(8,128)(2,1)S(1)}, u32[]{:S(2)}, u32[]{:S(2)}) %collective-permute-start.15) | collective-permute-done | bytes 524320 | tf_op jit(solution)/shard_map/ppermute | solution.py:378
  120.2 5.9 %collective-permute-done.20.refs_7_.refs_4_ = bf16[512,512]{1,0:T(8,128)(2,1)S(1)} collective-permute-done((bf16[512,512]{1,0:T(8,128)(2,1)S(1)}, bf16[512,512]{1,0:T(8,128)(2,1)S(1)}, u32[]{:S(2)}, u32[]{:S(2)}) %collective-permute-start.20) | collective-permute-done | bytes 524320 | tf_op jit(solution)/shard_map/ppermute | solution.py:378
  126.1 9.3 %collective-permute-done.21.refs_5_ = bf16[512,512]{1,0:T(8,128)(2,1)S(1)} collective-permute-done((bf16[512,512]{1,0:T(8,128)(2,1)S(1)}, bf16[512,512]{1,0:T(8,128)(2,1)S(1)}, u32[]{:S(2)}, u32[]{:S(2)}) %collective-permute-start.21) | collective-permute-done | bytes 524320 | tf_op jit(solution)/shard_map/ppermute | solution.py:378
  135.4 8.0 %shard_map.75 = (bf16[512,512]{1,0:T(8,128)(2,1)S(1)}, bf16[512,512]{1,0:T(8,128)(2,1)S(1)}, bf16[1024,512]{1,0:T(8,128)(2,1)S(1)}, bf16[1024,512]{1,0:T(8,128)(2,1)S(1)}) custom-call(s32[2]{0:T(128)S(1)} %pad_add_fusion.place_ref, f32[16,128]{1,0:T(8,128)S(1)} %copy-done.7, bf16[1024,1024]{1,0:T(8,128)(2,1)S(1)} %get-tuple-element.42.gate_ref, ...), custom_call_target="tpu_custom_call" | custom-call | flops 6442450944 | bytes 4194304 | tf_op jit(solution)/shard_map/pallas_call | solution.py:294
  143.4 8.0 %shard_map.76 = (bf16[512,512]{1,0:T(8,128)(2,1)S(1)}, bf16[512,512]{1,0:T(8,128)(2,1)S(1)}, bf16[512,512]{1,0:T(8,128)(2,1)S(1)}, bf16[512,512]{1,0:T(8,128)(2,...) custom-call(s32[2]{0:T(128)S(1)} %pad_add_fusion.place_ref, f32[16,128]{1,0:T(8,128)S(1)} %copy-done.7, ...), custom_call_target="tpu_custom_call" | custom-call | flops 6442450944 | bytes 4194304 | tf_op jit(solution)/shard_map/pallas_call | solution.py:294
  154.8 16.5 %collective-permute-done.24.refs_1_ = bf16[512,512]{1,0:T(8,128)(2,1)S(1)} collective-permute-done((bf16[512,512]{1,0:T(8,128)(2,1)S(1)}, bf16[512,512]{1,0:T(8,128)(2,1)S(1)}, u32[]{:S(2)}, u32[]{:S(2)}) %collective-permute-start.24) | collective-permute-done | bytes 524320 | tf_op jit(solution)/shard_map/ppermute | solution.py:378
  178.8 18.0 %collective-permute-done.32.refs_3_ = bf16[512,512]{1,0:T(8,128)(2,1)S(1)} collective-permute-done((bf16[512,512]{1,0:T(8,128)(2,1)S(1)}, bf16[512,512]{1,0:T(8,128)(2,1)S(1)}, u32[]{:S(2)}, u32[]{:S(2)}) %collective-permute-start.32) | collective-permute-done | bytes 524320 | tf_op jit(solution)/shard_map/ppermute | solution.py:378
  200.8 3.3 %collective-permute-done.29.refs_3_ = bf16[512,512]{1,0:T(8,128)(2,1)S(1)} collective-permute-done((bf16[512,512]{1,0:T(8,128)(2,1)S(1)}, bf16[512,512]{1,0:T(8,128)(2,1)S(1)}, u32[]{:S(2)}, u32[]{:S(2)}) %collective-permute-start.29) | collective-permute-done | bytes 524320 | tf_op jit(solution)/shard_map/ppermute | solution.py:378
  204.1 9.5 %collective-permute-done.33.refs_5_ = bf16[512,512]{1,0:T(8,128)(2,1)S(1)} collective-permute-done((bf16[512,512]{1,0:T(8,128)(2,1)S(1)}, bf16[512,512]{1,0:T(8,128)(2,1)S(1)}, u32[]{:S(2)}, u32[]{:S(2)}) %collective-permute-start.33) | collective-permute-done | bytes 524320 | tf_op jit(solution)/shard_map/ppermute | solution.py:378
  (86 shorter events, 56.3 us)
Async XLA Ops:
  2.6 15.3 %collective-permute-start = (bf16[3,64,1024]{2,1,0:T(8,128)(2,1)}, bf16[3,64,1024]{2,1,0:T(8,128)(2,1)S(1)}, u32[]{:S(2)}, u32[]{:S(2)}) collective-permute-start(bf16[3,64,1024]{2,1,0:T(8,128)(2,1)} %get-tuple-element.41.refs_0_), channel_id=1, source_target_pairs={{0,2},{1,3},{2,4},{3,5},{4,6},{5,7},{6,8},{7,9},{8,10},{9,11},{10,... | collective-permute-start | bytes 1179656 | tf_op jit(solution)/shard_map/ppermute | solution.py:385
  30.5 82.9 %collective-permute-start.8 = (bf16[3,320,1024]{2,1,0:T(8,128)(2,1)S(1)}, bf16[3,320,1024]{2,1,0:T(8,128)(2,1)}, u32[]{:S(2)}, u32[]{:S(2)}) collective-permute-start(bf16[3,320,1024]{2,1,0:T(8,128)(2,1)S(1)} %shard_map.73.refs_0_), channel_id=1, source_target_pairs={{0,1},{1,0},{2,3},{3,2},{4,5},{5,4},{6,7},{7,6},{8,9},{9,8},{10,11... | collective-permute-start | bytes 5898248 | tf_op jit(solution)/shard_map/ppermute | solution.py:389
  32.6 22.1 %collective-permute-start.10 = (bf16[512,512]{1,0:T(8,128)(2,1)S(1)}, bf16[512,512]{1,0:T(8,128)(2,1)S(1)}, u32[]{:S(2)}, u32[]{:S(2)}) collective-permute-start(bf16[512,512]{1,0:T(8,128)(2,1)S(1)} %copy-done.5), channel_id=1, source_target_pairs={{0,16},{16,32},{32,48},{48,0},{64,80},{80,96},{96,112},{112,64},{1... | collective-permute-start | bytes 1572872 | tf_op jit(solution)/shard_map/ppermute | solution.py:378
  36.4 15.4 %collective-permute-start.6 = (bf16[3,64,1024]{2,1,0:T(8,128)(2,1)S(1)}, bf16[3,64,1024]{2,1,0:T(8,128)(2,1)S(1)}, u32[]{:S(2)}, u32[]{:S(2)}) collective-permute-start(bf16[3,64,1024]{2,1,0:T(8,128)(2,1)S(1)} %collective-permute-done.2.refs_3_), channel_id=1, source_target_pairs={{0,2},{1,3},{2,4},{3,5},{4,6},{5,7},{6,8},{7,9},{8,10},{9,11},{10,... | collective-permute-start | bytes 1179656 | tf_op jit(solution)/shard_map/ppermute | solution.py:385
  54.6 58.8 %collective-permute-start.9 = (bf16[3,192,1024]{2,1,0:T(8,128)(2,1)S(1)}, bf16[3,192,1024]{2,1,0:T(8,128)(2,1)}, u32[]{:S(2)}, u32[]{:S(2)}) collective-permute-start(bf16[3,192,1024]{2,1,0:T(8,128)(2,1)S(1)} %shard_map.74.refs_1_), channel_id=1, source_target_pairs={{0,1},{1,0},{2,3},{3,2},{4,5},{5,4},{6,7},{7,6},{8,9},{9,8},{10,11... | collective-permute-start | bytes 3538952 | tf_op jit(solution)/shard_map/ppermute | solution.py:389
  57.0 31.3 %collective-permute-start.16 = (bf16[512,512]{1,0:T(8,128)(2,1)}, bf16[512,512]{1,0:T(8,128)(2,1)}, u32[]{:S(2)}, u32[]{:S(2)}) collective-permute-start(bf16[512,512]{1,0:T(8,128)(2,1)} %get-tuple-element.49.own_ref), channel_id=1, source_target_pairs={{0,64},{16,80},{32,96},{48,112},{64,128},{80,144},{96,160},{112,17... | collective-permute-start | bytes 1572872 | tf_op jit(solution)/shard_map/ppermute | solution.py:378
  58.9 31.9 %collective-permute-start.18 = (bf16[512,512]{1,0:T(8,128)(2,1)}, bf16[512,512]{1,0:T(8,128)(2,1)}, u32[]{:S(2)}, u32[]{:S(2)}) collective-permute-start(bf16[512,512]{1,0:T(8,128)(2,1)} %get-tuple-element.49.own_ref), channel_id=1, source_target_pairs={{0,192},{16,208},{32,224},{48,240},{64,0},{80,16},{96,32},{112,48}... | collective-permute-start | bytes 1572872 | tf_op jit(solution)/shard_map/ppermute | solution.py:378
  65.4 16.1 %collective-permute-start.13 = (bf16[256,512]{1,0:T(8,128)(2,1)}, bf16[256,512]{1,0:T(8,128)(2,1)}, u32[]{:S(2)}, u32[]{:S(2)}) collective-permute-start(bf16[256,512]{1,0:T(8,128)(2,1)} %slice.27), channel_id=1, source_target_pairs={{0,48},{16,0},{32,16},{48,32},{64,112},{80,64},{96,80},{112,96},{1... | collective-permute-start | bytes 786440 | tf_op jit(solution)/shard_map/ppermute | solution.py:378
  87.6 24.9 %collective-permute-start.14 = (bf16[512,512]{1,0:T(8,128)(2,1)S(1)}, bf16[512,512]{1,0:T(8,128)(2,1)S(1)}, u32[]{:S(2)}, u32[]{:S(2)}) collective-permute-start(bf16[512,512]{1,0:T(8,128)(2,1)S(1)} %get-tuple-element.46), channel_id=1, source_target_pairs={{0,64},{16,80},{32,96},{48,112},{64,128},{80,144},{96,160},{112,17... | collective-permute-start | bytes 1572872 | tf_op jit(solution)/shard_map/ppermute | solution.py:378
  89.3 15.9 %collective-permute-start.17 = (bf16[256,512]{1,0:T(8,128)(2,1)S(1)}, bf16[256,512]{1,0:T(8,128)(2,1)S(1)}, u32[]{:S(2)}, u32[]{:S(2)}) collective-permute-start(bf16[256,512]{1,0:T(8,128)(2,1)S(1)} %slice.28), channel_id=1, source_target_pairs={{0,64},{16,80},{32,96},{48,112},{64,128},{80,144},{96,160},{112,17... | collective-permute-start | bytes 786440 | tf_op jit(solution)/shard_map/ppermute | solution.py:378
  91.8 16.1 %collective-permute-start.19 = (bf16[256,512]{1,0:T(8,128)(2,1)S(1)}, bf16[256,512]{1,0:T(8,128)(2,1)S(1)}, u32[]{:S(2)}, u32[]{:S(2)}) collective-permute-start(bf16[256,512]{1,0:T(8,128)(2,1)S(1)} %slice.29), channel_id=1, source_target_pairs={{0,192},{16,208},{32,224},{48,240},{64,0},{80,16},{96,32},{112,48}... | collective-permute-start | bytes 786440 | tf_op jit(solution)/shard_map/ppermute | solution.py:378
  112.5 22.9 %collective-permute-start.21 = (bf16[512,512]{1,0:T(8,128)(2,1)S(1)}, bf16[512,512]{1,0:T(8,128)(2,1)S(1)}, u32[]{:S(2)}, u32[]{:S(2)}) collective-permute-start(bf16[512,512]{1,0:T(8,128)(2,1)S(1)} %get-tuple-element.52), channel_id=1, source_target_pairs={{0,16},{16,32},{32,48},{48,0},{64,80},{80,96},{96,112},{112,64},{1... | collective-permute-start | bytes 1572872 | tf_op jit(solution)/shard_map/ppermute | solution.py:378
  113.4 22.0 %collective-permute-start.22 = (bf16[512,512]{1,0:T(8,128)(2,1)S(1)}, bf16[512,512]{1,0:T(8,128)(2,1)S(1)}, u32[]{:S(2)}, u32[]{:S(2)}) collective-permute-start(bf16[512,512]{1,0:T(8,128)(2,1)S(1)} %get-tuple-element.53), channel_id=1, source_target_pairs={{0,128},{16,144},{32,160},{48,176},{64,192},{80,208},{96,224},{112... | collective-permute-start | bytes 1572872 | tf_op jit(solution)/shard_map/ppermute | solution.py:378
  113.4 22.0 %collective-permute-start.23 = (bf16[512,512]{1,0:T(8,128)(2,1)S(1)}, bf16[512,512]{1,0:T(8,128)(2,1)S(1)}, u32[]{:S(2)}, u32[]{:S(2)}) collective-permute-start(bf16[512,512]{1,0:T(8,128)(2,1)S(1)} %get-tuple-element.54), channel_id=1, source_target_pairs={{0,32},{16,48},{32,0},{48,16},{64,96},{80,112},{96,64},{112,80},{1... | collective-permute-start | bytes 1572872 | tf_op jit(solution)/shard_map/ppermute | solution.py:378
  151.4 19.8 %collective-permute-start.24 = (bf16[512,512]{1,0:T(8,128)(2,1)S(1)}, bf16[512,512]{1,0:T(8,128)(2,1)S(1)}, u32[]{:S(2)}, u32[]{:S(2)}) collective-permute-start(bf16[512,512]{1,0:T(8,128)(2,1)S(1)} %get-tuple-element.58), channel_id=1, source_target_pairs={{0,192},{16,208},{32,224},{48,240},{64,0},{80,16},{96,32},{112,48}... | collective-permute-start | bytes 1572872 | tf_op jit(solution)/shard_map/ppermute | solution.py:378
  151.8 19.5 %collective-permute-start.25 = (bf16[512,512]{1,0:T(8,128)(2,1)S(1)}, bf16[512,512]{1,0:T(8,128)(2,1)S(1)}, u32[]{:S(2)}, u32[]{:S(2)}) collective-permute-start(bf16[512,512]{1,0:T(8,128)(2,1)S(1)} %get-tuple-element.59), channel_id=1, source_target_pairs={{0,128},{16,144},{32,160},{48,176},{64,192},{80,208},{96,224},{112... | collective-permute-start | bytes 1572872 | tf_op jit(solution)/shard_map/ppermute | solution.py:378
  152.3 20.8 %collective-permute-start.26 = (bf16[512,512]{1,0:T(8,128)(2,1)S(1)}, bf16[512,512]{1,0:T(8,128)(2,1)S(1)}, u32[]{:S(2)}, u32[]{:S(2)}) collective-permute-start(bf16[512,512]{1,0:T(8,128)(2,1)S(1)} %get-tuple-element.60), channel_id=1, source_target_pairs={{0,64},{16,80},{32,96},{48,112},{64,128},{80,144},{96,160},{112,17... | collective-permute-start | bytes 1572872 | tf_op jit(solution)/shard_map/ppermute | solution.py:378
  153.7 23.9 %collective-permute-start.30 = (bf16[512,512]{1,0:T(8,128)(2,1)S(1)}, bf16[512,512]{1,0:T(8,128)(2,1)S(1)}, u32[]{:S(2)}, u32[]{:S(2)}) collective-permute-start(bf16[512,512]{1,0:T(8,128)(2,1)S(1)} %get-tuple-element.66), channel_id=1, source_target_pairs={{0,48},{16,0},{32,16},{48,32},{64,112},{80,64},{96,80},{112,96},{1... | collective-permute-start | bytes 1572872 | tf_op jit(solution)/shard_map/ppermute | solution.py:378
  154.1 24.7 %collective-permute-start.31 = (bf16[512,512]{1,0:T(8,128)(2,1)S(1)}, bf16[512,512]{1,0:T(8,128)(2,1)S(1)}, u32[]{:S(2)}, u32[]{:S(2)}) collective-permute-start(bf16[512,512]{1,0:T(8,128)(2,1)S(1)} %get-tuple-element.67), channel_id=1, source_target_pairs={{0,32},{16,48},{32,0},{48,16},{64,96},{80,112},{96,64},{112,80},{1... | collective-permute-start | bytes 1572872 | tf_op jit(solution)/shard_map/ppermute | solution.py:378
  171.3 25.5 %collective-permute-start.32 = (bf16[512,512]{1,0:T(8,128)(2,1)S(1)}, bf16[512,512]{1,0:T(8,128)(2,1)S(1)}, u32[]{:S(2)}, u32[]{:S(2)}) collective-permute-start(bf16[512,512]{1,0:T(8,128)(2,1)S(1)} %get-tuple-element.68), channel_id=1, source_target_pairs={{0,16},{16,32},{32,48},{48,0},{64,80},{80,96},{96,112},{112,64},{1... | collective-permute-start | bytes 1572872 | tf_op jit(solution)/shard_map/ppermute | solution.py:378
  175.1 23.8 %collective-permute-start.27 = (bf16[512,512]{1,0:T(8,128)(2,1)S(1)}, bf16[512,512]{1,0:T(8,128)(2,1)S(1)}, u32[]{:S(2)}, u32[]{:S(2)}) collective-permute-start(bf16[512,512]{1,0:T(8,128)(2,1)S(1)} %get-tuple-element.62), channel_id=1, source_target_pairs={{0,48},{16,0},{32,16},{48,32},{64,112},{80,64},{96,80},{112,96},{1... | collective-permute-start | bytes 1572872 | tf_op jit(solution)/shard_map/ppermute | solution.py:378
  177.0 23.8 %collective-permute-start.28 = (bf16[512,512]{1,0:T(8,128)(2,1)S(1)}, bf16[512,512]{1,0:T(8,128)(2,1)S(1)}, u32[]{:S(2)}, u32[]{:S(2)}) collective-permute-start(bf16[512,512]{1,0:T(8,128)(2,1)S(1)} %get-tuple-element.63), channel_id=1, source_target_pairs={{0,32},{16,48},{32,0},{48,16},{64,96},{80,112},{96,64},{112,80},{1... | collective-permute-start | bytes 1572872 | tf_op jit(solution)/shard_map/ppermute | solution.py:378
  177.5 26.6 %collective-permute-start.29 = (bf16[512,512]{1,0:T(8,128)(2,1)S(1)}, bf16[512,512]{1,0:T(8,128)(2,1)S(1)}, u32[]{:S(2)}, u32[]{:S(2)}) collective-permute-start(bf16[512,512]{1,0:T(8,128)(2,1)S(1)} %get-tuple-element.64), channel_id=1, source_target_pairs={{0,16},{16,32},{32,48},{48,0},{64,80},{80,96},{96,112},{112,64},{1... | collective-permute-start | bytes 1572872 | tf_op jit(solution)/shard_map/ppermute | solution.py:378
  198.9 16.8 %collective-permute-start.35 = (bf16[512,512]{1,0:T(8,128)(2,1)S(1)}, bf16[512,512]{1,0:T(8,128)(2,1)S(1)}, u32[]{:S(2)}, u32[]{:S(2)}) collective-permute-start(bf16[512,512]{1,0:T(8,128)(2,1)S(1)} %get-tuple-element.72), channel_id=1, source_target_pairs={{0,64},{16,80},{32,96},{48,112},{64,128},{80,144},{96,160},{112,17... | collective-permute-start | bytes 1572872 | tf_op jit(solution)/shard_map/ppermute | solution.py:378
  (21 other events, 196.5 us)

commit v2 on v1

--- a/solution.py
+++ b/solution.py
@@ -106,53 +106,56 @@
     )(stream, norm_gain.reshape(1, features), *parts)
 
 
-def pick_kernel(along_y, place_ref, rows_ref, own_ref, after_ref, top_ref, bottom_ref, before_ref, *refs):
-    outs = refs[:SIDE]
-    across_ref, chosen_ref = refs[SIDE:]
+def pick_kernel(place_ref, rows_ref, *refs):
+    count = SIDE + 1
+    across_ref, chosen_ref = refs[-2:]
     y, x = place_ref[0], place_ref[1]
-    tokens, half = own_ref.shape
     slots = rows_ref.shape[2]
-    across_ref[: tokens // 2, :] = top_ref[...]
-    across_ref[tokens // 2 :, :] = bottom_ref[...]
-    token = lax.broadcasted_iota(jnp.int32, (slots, tokens), 1).astype(jnp.float32)
-    for d in range(SIDE):
-        e = wrap(y + d) * SIDE + x if along_y else y * SIDE + wrap(x + d)
-        column = rows_ref[e].astype(jnp.float32).T
-        for t in range(SIDE):
-            k = t if along_y else SIDE + t
-            chosen_ref[t, d * slots : (d + 1) * slots, :] = jnp.where(column[:, k : k + 1] == token, 1.0, 0.0).astype(
-                jnp.bfloat16
-            )
-    step = half // 2
-
-    def work(i, carry):
-        at = pl.ds(pl.multiple_of(i * step, step), step)
-        for t, source in enumerate((own_ref, after_ref, across_ref, before_ref)):
-            rows = jnp.dot(chosen_ref[t], source[:, at], preferred_element_type=jnp.float32).astype(jnp.bfloat16)
-            for d in range(SIDE):
-                outs[d][t * slots : (t + 1) * slots, at] = rows[d * slots : (d + 1) * slots, :]
-        return carry
-
-    lax.fori_loop(0, 2, work, 0)
-
-
-def pick(along_y, place, rows, sources):
-    tokens, half = sources[0].shape
+    for along_y in (True, False):
+        own_ref, after_ref, top_ref, bottom_ref, before_ref = refs[:count] if along_y else refs[count : 2 * count]
+        outs = refs[2 * count :][:SIDE] if along_y else refs[2 * count + SIDE :][:SIDE]
+        tokens, half = own_ref.shape
+        across_ref[: tokens // 2, :] = top_ref[...]
+        across_ref[tokens // 2 :, :] = bottom_ref[...]
+        token = lax.broadcasted_iota(jnp.int32, (slots, tokens), 1).astype(jnp.float32)
+        for d in range(SIDE):
+            e = wrap(y + d) * SIDE + x if along_y else y * SIDE + wrap(x + d)
+            column = rows_ref[e].astype(jnp.float32).T
+            for t in range(SIDE):
+                k = t if along_y else SIDE + t
+                chosen_ref[t, d * slots : (d + 1) * slots, :] = jnp.where(
+                    column[:, k : k + 1] == token, 1.0, 0.0
+                ).astype(jnp.bfloat16)
+        step = half // 2
+
+        def work(i, carry, outs=outs, sources=(own_ref, after_ref, across_ref, before_ref), step=step):
+            at = pl.ds(pl.multiple_of(i * step, step), step)
+            for t, source in enumerate(sources):
+                rows = jnp.dot(chosen_ref[t], source[:, at], preferred_element_type=jnp.float32).astype(jnp.bfloat16)
+                for d in range(SIDE):
+                    outs[d][t * slots : (t + 1) * slots, at] = rows[d * slots : (d + 1) * slots, :]
+            return carry
+
+        lax.fori_loop(0, 2, work, 0)
+
+
+def pick(place, rows, lows, highs):
+    tokens, half = lows[0].shape
     slots = rows.shape[2]
     return pl.pallas_call(
-        functools.partial(pick_kernel, along_y),
-        in_specs=[SMEM] + [VMEM] * 6,
-        out_shape=[jax.ShapeDtypeStruct((SIDE * slots, half), jnp.bfloat16)] * SIDE,
+        pick_kernel,
+        in_specs=[SMEM] + [VMEM] * (1 + len(lows) + len(highs)),
+        out_shape=[jax.ShapeDtypeStruct((SIDE * slots, half), jnp.bfloat16)] * (2 * SIDE),
         scratch_shapes=[
             pltpu.VMEM((tokens, half), jnp.bfloat16),
             pltpu.VMEM((SIDE, SIDE * slots, tokens), jnp.bfloat16),
         ],
         cost_estimate=pl.CostEstimate(
-            flops=2 * SIDE * SIDE * slots * tokens * half, bytes_accessed=4 << 20, transcendentals=0
-        ),
-        compiler_params=pltpu.CompilerParams(vmem_limit_bytes=14 << 20),
-        name="pick_y" if along_y else "pick_x",
-    )(place, rows, *sources)
+            flops=4 * SIDE * SIDE * slots * tokens * half, bytes_accessed=8 << 20, transcendentals=0
+        ),
+        compiler_params=pltpu.CompilerParams(vmem_limit_bytes=20 << 20),
+        name="pick",
+    )(place, rows, *lows, *highs)
 
 
 def stack_kernel(*refs):
@@ -310,42 +313,46 @@
     return {name[1:]: array for name, array in results.items() if name[0] == "out"}
 
 
-def relay_kernel(along_y, place_ref, rows_ref, *refs):
-    pieces, outs = refs[:SIDE], refs[SIDE:]
+def relay_kernel(place_ref, rows_ref, *refs):
     y, x = place_ref[0], place_ref[1]
-    tokens, slots = outs[0].shape[0], rows_ref.shape[2]
+    tokens, slots = refs[-1].shape[0], rows_ref.shape[2]
     step = tokens // 2
     token = lax.broadcasted_iota(jnp.int32, (step, slots), 0)
-    lists = []
-    for d in range(SIDE):
-        lists.append(rows_ref[wrap(y + d) * SIDE + x if along_y else y * SIDE + wrap(x + d)])
-
-    def work(i, carry):
-        for t in range(SIDE):
-            k = t if along_y else SIDE + t
-            chosen = jnp.concatenate(
-                [jnp.where(token + i * step == rows[k : k + 1, :], 1.0, 0.0).astype(jnp.bfloat16) for rows in lists], 1
-            )
-            rows = jnp.concatenate([piece[t * slots : (t + 1) * slots, :] for piece in pieces])
-            total = jnp.dot(chosen, rows, preferred_element_type=jnp.float32)
-            outs[t][pl.ds(pl.multiple_of(i * step, step), step), :] = total.astype(jnp.bfloat16)
-        return carry
-
-    lax.fori_loop(0, 2, work, 0)
-
-
-def relay(along_y, place, rows, pieces, tokens):
-    total, half = pieces[0].shape
-    return pl.pallas_call(
-        functools.partial(relay_kernel, along_y),
-        in_specs=[SMEM] + [VMEM] * (1 + SIDE),
-        out_shape=[jax.ShapeDtypeStruct((tokens, half), jnp.bfloat16)] * SIDE,
+    for along_y in (True, False):
+        first = 0 if along_y else SIDE
+        pieces, outs = refs[first : first + SIDE], refs[first + 2 * SIDE : first + 3 * SIDE]
+        lists = [rows_ref[wrap(y + d) * SIDE + x if along_y else y * SIDE + wrap(x + d)] for d in range(SIDE)]
+
+        def work(i, carry, first=first, pieces=pieces, outs=outs, lists=lists):
+            for t in range(SIDE):
+                k = first + t
+                chosen = jnp.concatenate(
+                    [
+                        jnp.where(token + i * step == rows[k : k + 1, :], 1.0, 0.0).astype(jnp.bfloat16)
+                        for rows in lists
+                    ],
+                    1,
+                )
+                rows = jnp.concatenate([piece[t * slots : (t + 1) * slots, :] for piece in pieces])
+                total = jnp.dot(chosen, rows, preferred_element_type=jnp.float32)
+                outs[t][pl.ds(pl.multiple_of(i * step, step), step), :] = total.astype(jnp.bfloat16)
+            return carry
+
+        lax.fori_loop(0, 2, work, 0)
+
+
+def relay(place, rows, lows, highs, tokens):
+    total, half = lows[0].shape
+    return pl.pallas_call(
+        relay_kernel,
+        in_specs=[SMEM] + [VMEM] * (1 + len(lows) + len(highs)),
+        out_shape=[jax.ShapeDtypeStruct((tokens, half), jnp.bfloat16)] * (2 * SIDE),
         cost_estimate=pl.CostEstimate(
-            flops=2 * SIDE * total * tokens * half, bytes_accessed=4 << 20, transcendentals=0
-        ),
-        compiler_params=pltpu.CompilerParams(vmem_limit_bytes=12 << 20),
-        name="relay_y" if along_y else "relay_x",
-    )(place, rows, *pieces)
+            flops=4 * SIDE * total * tokens * half, bytes_accessed=8 << 20, transcendentals=0
+        ),
+        compiler_params=pltpu.CompilerParams(vmem_limit_bytes=16 << 20),
+        name="relay",
+    )(place, rows, *lows, *highs)
 
 
 def add_kernel(*refs):
@@ -407,10 +414,11 @@
     lows = [low, left, over_plane(left[:mid], 0, 1), over_plane(right[mid:], 0, -1), right]
     highs = [high, down, over_plane(down[:mid], 1, 0), over_plane(up[mid:], -1, 0), up]
     ahead2, behind2 = along_z(ahead, 1, tp_count), along_z(behind, -1, tp_count)
-    picked_low = pick(True, place, rows_here, lows)
-    arrived_low = [picked_low[0]] + [over_plane(picked_low[d], d, 0) for d in range(1, SIDE)]
-    picked_high = pick(False, place, rows_here, highs)
-    arrived_high = [picked_high[0]] + [over_plane(picked_high[d], 0, d) for d in range(1, SIDE)]
+    picked = pick(place, rows_here, lows, highs)
+    arrived_low, arrived_high = [picked[0]] + [None] * (SIDE - 1), [picked[SIDE]] + [None] * (SIDE - 1)
+    for d in (1, 3, 2):
+        arrived_low[d] = over_plane(picked[d], d, 0)
+        arrived_high[d] = over_plane(picked[SIDE + d], 0, d)
     cut = own.shape[1] // 2
     far = [
         along_z(ahead2[:, :cut], 2, tp_count),
@@ -432,11 +440,13 @@
                 back[half, by] = over_plane(piece, -by, 0)
             else:
                 back[half, by] = over_plane(piece, 0, -by)
-    sums_low = relay(True, place, rows_here, [back["low", d] for d in range(SIDE)], block)
-    sums_low = [sums_low[0]] + [over_plane(sums_low[t], 0, -t) for t in range(1, SIDE)]
-    sums_high = relay(False, place, rows_here, [back["high", d] for d in range(SIDE)], block)
-    sums_high = [sums_high[0]] + [over_plane(sums_high[t], -t, 0) for t in range(1, SIDE)]
-    return add(sums_low, sums_high)
+    lows, highs = [back["low", d] for d in range(SIDE)], [back["high", d] for d in range(SIDE)]
+    sums = relay(place, rows_here, lows, highs, block)
+    lows, highs = [sums[0]], [sums[SIDE]]
+    for t in (1, 3, 2):
+        lows.append(over_plane(sums[t], 0, -t))
+        highs.append(over_plane(sums[SIDE + t], -t, 0))
+    return add(lows, highs)
 
 
 def solution(mesh):

time: 218 us -> 207 us (0.950)
  the two profiles are of different devices: /device:TPU:8 before, /device:TPU:4 now
where the time goes in v2:
time: 207 us
  waiting for transfers between devices  109 us (53%)
  starting transfers between devices  53.7 us (26%)
  Pallas kernels  34.1 us (16%)
  local copies, waits for them, and re-layouts  9.54 us (5%)
    ppermute x26, waiting for transfers between devices, over_plane(): lax.ppermute(array, 'ep', [(y * SIDE + x, (y + by_y) % SIDE * SIDE + (x +...  62.9 us
    ppermute x8, waiting for transfers between devices, along_z(): lax.ppermute(array, 'tp', [(z * 2 + c, (z + by) % chips * 2 + c) for z in...  40.1 us
    ppermute x26, starting transfers between devices, over_plane(): lax.ppermute(array, 'ep', [(y * SIDE + x, (y + by_y) % SIDE * SIDE + (x +...  33.6 us
    pallas_call x2, Pallas kernels, expert(): pl.pallas_call(functools.partial(expert_kernel, number, [*inputs, *outs])...  16 us
    ppermute x8, starting transfers between devices, along_z(): lax.ppermute(array, 'tp', [(z * 2 + c, (z + by) % chips * 2 + c) for z in...  14.3 us
    unnamed x28, local copies, waits for them, and re-layouts  7.26 us
    all_to_all x1, starting transfers between devices, layer(): lax.all_to_all(rows_there, 'ep', split_axis=0, concat_axis=0, tiled=True)  5.57 us
    all_to_all x1, waiting for transfers between devices, layer(): lax.all_to_all(rows_there, 'ep', split_axis=0, concat_axis=0, tiled=True)  5.52 us
  transfers between devices with their start and end apart: 37, of which 19 were waited for; matrix products, arithmetic and copies ran while one was open for 1% of the time, Pallas kernels for 5%

profile of v2, /device:TPU:4, one launch (start us, length us, event | category | flops | bytes accessed | tf_op | source)
XLA Modules:
  0.0 206.6 jit_solution(16423006369954890936)
XLA Ops:
  4.6 4.0 %collective-permute-start.1 = (bf16[3,64,1024]{2,1,0:T(8,128)(2,1)}, bf16[3,64,1024]{2,1,0:T(8,128)(2,1)S(1)}, u32[]{:S(2)}, u32[]{:S(2)}) collective-permute-start(bf16[3,64,1024]{2,1,0:T(8,128)(2,1)} %get-tuple-element.41.refs_0_), channel_id=1, source_target_pairs={{0,14},{1,15},{2,0},{3,1},{4,2},{5,3},{6,4},{7,5},{8,6},{9,7},{10,... | collective-permute-start | bytes 1179656 | tf_op jit(solution)/shard_map/ppermute | solution.py:392
  8.6 9.2 %collective-permute-done.refs_1_ = bf16[3,64,1024]{2,1,0:T(8,128)(2,1)S(1)} collective-permute-done((bf16[3,64,1024]{2,1,0:T(8,128)(2,1)}, bf16[3,64,1024]{2,1,0:T(8,128)(2,1)S(1)}, u32[]{:S(2)}, u32[]{:S(2)}) %collective-permute-start) | collective-permute-done | bytes 393248 | tf_op jit(solution)/shard_map/ppermute | solution.py:392
  17.9 3.2 %collective-permute-start.3 = (bf16[3,64,1024]{2,1,0:T(8,128)(2,1)S(1)}, bf16[3,64,1024]{2,1,0:T(8,128)(2,1)S(1)}, u32[]{:S(2)}, u32[]{:S(2)}) collective-permute-start(bf16[3,64,1024]{2,1,0:T(8,128)(2,1)S(1)} %collective-permute-done.1.refs_2_), channel_id=1, source_target_pairs={{0,14},{1,15},{2,0},{3,1},{4,2},{5,3},{6,4},{7,5},{8,6},{9,7},{10,... | collective-permute-start | bytes 1179656 | tf_op jit(solution)/shard_map/ppermute | solution.py:392
  22.3 7.1 %collective-permute-done.2.refs_3_ = bf16[3,64,1024]{2,1,0:T(8,128)(2,1)S(1)} collective-permute-done((bf16[3,64,1024]{2,1,0:T(8,128)(2,1)S(1)}, bf16[3,64,1024]{2,1,0:T(8,128)(2,1)S(1)}, u32[]{:S(2)}, u32[]{:S(2)}) %collective-permute-start.2) | collective-permute-done | bytes 393248 | tf_op jit(solution)/shard_map/ppermute | solution.py:392
  30.7 4.9 %collective-permute-start.4 = (bf16[3,32,1024]{2,1,0:T(8,128)(2,1)S(1)}, bf16[3,32,1024]{2,1,0:T(8,128)(2,1)S(1)}, u32[]{:S(2)}, u32[]{:S(2)}) collective-permute-start(bf16[3,32,1024]{2,1,0:T(8,128)(2,1)S(1)} %slice.24), channel_id=1, source_target_pairs={{0,4},{1,5},{2,6},{3,7},{4,8},{5,9},{6,10},{7,11},{8,12},{9,13},{1... | collective-permute-start | bytes 589832 | tf_op jit(solution)/shard_map/ppermute | solution.py:392
  36.4 16.6 %collective-permute-done.4.refs_0_ = bf16[3,32,1024]{2,1,0:T(8,128)(2,1)S(1)} collective-permute-done((bf16[3,32,1024]{2,1,0:T(8,128)(2,1)S(1)}, bf16[3,32,1024]{2,1,0:T(8,128)(2,1)S(1)}, u32[]{:S(2)}, u32[]{:S(2)}) %collective-permute-start.4) | collective-permute-done | bytes 196640 | tf_op jit(solution)/shard_map/ppermute | solution.py:392
  56.3 7.2 %collective-permute-done.7.refs_3_ = bf16[3,64,1024]{2,1,0:T(8,128)(2,1)S(1)} collective-permute-done((bf16[3,64,1024]{2,1,0:T(8,128)(2,1)S(1)}, bf16[3,64,1024]{2,1,0:T(8,128)(2,1)S(1)}, u32[]{:S(2)}, u32[]{:S(2)}) %collective-permute-start.7) | collective-permute-done | bytes 393248 | tf_op jit(solution)/shard_map/ppermute | solution.py:392
  76.5 5.6 %all-to-all-start = ((s32[16,8,128]{2,1,0:T(8,128)}), s32[16,8,128]{2,1,0:T(8,128)S(1)}, u32[]{:S(2)}, u32[]{:S(2)}) async-start(s32[16,8,128]{2,1,0:T(8,128)} %get-tuple-element.39), calls=%async_computation | async-start | bytes 131072 | tf_op jit(solution)/shard_map/all_to_all | solution.py:412
  82.1 5.5 %all-to-all-done.rows_ref = s32[16,8,128]{2,1,0:T(8,128)S(1)} async-done(((s32[16,8,128]{2,1,0:T(8,128)}), s32[16,8,128]{2,1,0:T(8,128)S(1)}, u32[]{:S(2)}, u32[]{:S(2)}) %all-to-all-start) | async-done | bytes 65568 | tf_op jit(solution)/shard_map/all_to_all | solution.py:412
  93.9 5.1 %pick.1 = (bf16[512,512]{1,0:T(8,128)(2,1)S(1)}, bf16[512,512]{1,0:T(8,128)(2,1)S(1)}, bf16[512,512]{1,0:T(8,128)(2,1)S(1)}, bf16[512,512]{1,0:T(8,128)(2,1)S(1)...) custom-call(s32[2]{0:T(128)S(1)} %pad_add_fusion.place_ref, ...), custom_call_target="tpu_custom_call" | custom-call | flops 2147483648 | bytes 8388608 | tf_op jit(solution)/shard_map/pick/pallas_call | solution.py:145
  103.7 7.2 %collective-permute-done.18.refs_2_.refs_0_ = bf16[512,512]{1,0:T(8,128)(2,1)S(1)} collective-permute-done((bf16[512,512]{1,0:T(8,128)(2,1)S(1)}, bf16[512,512]{1,0:T(8,128)(2,1)S(1)}, u32[]{:S(2)}, u32[]{:S(2)}) %collective-permute-start.18) | collective-permute-done | bytes 524320 | tf_op jit(solution)/shard_map/ppermute | solution.py:385
  116.5 5.0 %collective-permute-done.19.refs_3_.refs_2_ = bf16[512,512]{1,0:T(8,128)(2,1)S(1)} collective-permute-done((bf16[512,512]{1,0:T(8,128)(2,1)S(1)}, bf16[512,512]{1,0:T(8,128)(2,1)S(1)}, u32[]{:S(2)}, u32[]{:S(2)}) %collective-permute-start.19) | collective-permute-done | bytes 524320 | tf_op jit(solution)/shard_map/ppermute | solution.py:385
  121.5 3.5 %collective-permute-done.21.refs_5_ = bf16[512,512]{1,0:T(8,128)(2,1)S(1)} collective-permute-done((bf16[512,512]{1,0:T(8,128)(2,1)S(1)}, bf16[512,512]{1,0:T(8,128)(2,1)S(1)}, u32[]{:S(2)}, u32[]{:S(2)}) %collective-permute-start.21) | collective-permute-done | bytes 524320 | tf_op jit(solution)/shard_map/ppermute | solution.py:385
  124.9 7.7 %collective-permute-done.23.refs_6_ = bf16[512,512]{1,0:T(8,128)(2,1)S(1)} collective-permute-done((bf16[512,512]{1,0:T(8,128)(2,1)S(1)}, bf16[512,512]{1,0:T(8,128)(2,1)S(1)}, u32[]{:S(2)}, u32[]{:S(2)}) %collective-permute-start.23) | collective-permute-done | bytes 524320 | tf_op jit(solution)/shard_map/ppermute | solution.py:385
  132.7 8.0 %shard_map.75 = (bf16[512,512]{1,0:T(8,128)(2,1)S(1)}, bf16[512,512]{1,0:T(8,128)(2,1)S(1)}, bf16[1024,512]{1,0:T(8,128)(2,1)S(1)}, bf16[1024,512]{1,0:T(8,128)(2,1)S(1)}) custom-call(s32[2]{0:T(128)S(1)} %pad_add_fusion.place_ref, f32[16,128]{1,0:T(8,128)S(1)} %copy-done.13, bf16[1024,1024]{1,0:T(8,128)(2,1)S(1)} %get-tuple-element.42.gate_ref, ...), custom_call_target="tpu_custom_call" | custom-call | flops 6442450944 | bytes 4194304 | tf_op jit(solution)/shard_map/pallas_call | solution.py:297
  140.7 8.0 %shard_map.76 = (bf16[512,512]{1,0:T(8,128)(2,1)S(1)}, bf16[512,512]{1,0:T(8,128)(2,1)S(1)}, bf16[512,512]{1,0:T(8,128)(2,1)S(1)}, bf16[512,512]{1,0:T(8,128)(2,...) custom-call(s32[2]{0:T(128)S(1)} %pad_add_fusion.place_ref, f32[16,128]{1,0:T(8,128)S(1)} %copy-done.13, ...), custom_call_target="tpu_custom_call" | custom-call | flops 6442450944 | bytes 4194304 | tf_op jit(solution)/shard_map/pallas_call | solution.py:297
  153.5 9.8 %collective-permute-done.24.refs_1_ = bf16[512,512]{1,0:T(8,128)(2,1)S(1)} collective-permute-done((bf16[512,512]{1,0:T(8,128)(2,1)S(1)}, bf16[512,512]{1,0:T(8,128)(2,1)S(1)}, u32[]{:S(2)}, u32[]{:S(2)}) %collective-permute-start.24) | collective-permute-done | bytes 524320 | tf_op jit(solution)/shard_map/ppermute | solution.py:385
  164.9 5.6 %collective-permute-done.26.refs_3_ = bf16[512,512]{1,0:T(8,128)(2,1)S(1)} collective-permute-done((bf16[512,512]{1,0:T(8,128)(2,1)S(1)}, bf16[512,512]{1,0:T(8,128)(2,1)S(1)}, u32[]{:S(2)}, u32[]{:S(2)}) %collective-permute-start.26) | collective-permute-done | bytes 524320 | tf_op jit(solution)/shard_map/ppermute | solution.py:385
  172.5 3.4 %relay.1 = (bf16[512,512]{1,0:T(8,128)(2,1)S(1)}, bf16[512,512]{1,0:T(8,128)(2,1)S(1)}, bf16[512,512]{1,0:T(8,128)(2,1)S(1)}, bf16[512,512]{1,0:T(8,128)(2,1)S(1...) custom-call(s32[2]{0:T(128)S(1)} %pad_add_fusion.place_ref, ...), custom_call_target="tpu_custom_call" | custom-call | flops 2147483648 | bytes 8388608 | tf_op jit(solution)/shard_map/relay/pallas_call | solution.py:346
  178.0 3.3 %collective-permute-start.32 = (bf16[512,512]{1,0:T(8,128)(2,1)S(1)}, bf16[512,512]{1,0:T(8,128)(2,1)S(1)}, u32[]{:S(2)}, u32[]{:S(2)}) collective-permute-start(bf16[512,512]{1,0:T(8,128)(2,1)S(1)} %get-tuple-element.68), channel_id=1, source_target_pairs={{0,32},{16,48},{32,0},{48,16},{64,96},{80,112},{96,64},{112,80},{1... | collective-permute-start | bytes 1572872 | tf_op jit(solution)/shard_map/ppermute | solution.py:385
  183.4 7.4 %collective-permute-done.30.refs_1_ = bf16[512,512]{1,0:T(8,128)(2,1)S(1)} collective-permute-done((bf16[512,512]{1,0:T(8,128)(2,1)S(1)}, bf16[512,512]{1,0:T(8,128)(2,1)S(1)}, u32[]{:S(2)}, u32[]{:S(2)}) %collective-permute-start.30) | collective-permute-done | bytes 524320 | tf_op jit(solution)/shard_map/ppermute | solution.py:385
  190.7 3.3 %collective-permute-start.35 = (bf16[512,512]{1,0:T(8,128)(2,1)S(1)}, bf16[512,512]{1,0:T(8,128)(2,1)S(1)}, u32[]{:S(2)}, u32[]{:S(2)}) collective-permute-start(bf16[512,512]{1,0:T(8,128)(2,1)S(1)} %get-tuple-element.72), channel_id=1, source_target_pairs={{0,128},{16,144},{32,160},{48,176},{64,192},{80,208},{96,224},{112... | collective-permute-start | bytes 1572872 | tf_op jit(solution)/shard_map/ppermute | solution.py:385
  194.0 5.6 %collective-permute-done.32.refs_3_ = bf16[512,512]{1,0:T(8,128)(2,1)S(1)} collective-permute-done((bf16[512,512]{1,0:T(8,128)(2,1)S(1)}, bf16[512,512]{1,0:T(8,128)(2,1)S(1)}, u32[]{:S(2)}, u32[]{:S(2)}) %collective-permute-start.32) | collective-permute-done | bytes 524320 | tf_op jit(solution)/shard_map/ppermute | solution.py:385
  200.4 4.4 %collective-permute-done.34.refs_6_ = bf16[512,512]{1,0:T(8,128)(2,1)S(1)} collective-permute-done((bf16[512,512]{1,0:T(8,128)(2,1)S(1)}, bf16[512,512]{1,0:T(8,128)(2,1)S(1)}, u32[]{:S(2)}, u32[]{:S(2)}) %collective-permute-start.34) | collective-permute-done | bytes 524320 | tf_op jit(solution)/shard_map/ppermute | solution.py:385
  (96 shorter events, 55.8 us)
Async XLA Ops:
  2.6 15.3 %collective-permute-start = (bf16[3,64,1024]{2,1,0:T(8,128)(2,1)}, bf16[3,64,1024]{2,1,0:T(8,128)(2,1)S(1)}, u32[]{:S(2)}, u32[]{:S(2)}) collective-permute-start(bf16[3,64,1024]{2,1,0:T(8,128)(2,1)} %get-tuple-element.41.refs_0_), channel_id=1, source_target_pairs={{0,2},{1,3},{2,4},{3,5},{4,6},{5,7},{6,8},{7,9},{8,10},{9,11},{10,... | collective-permute-start | bytes 1179656 | tf_op jit(solution)/shard_map/ppermute | solution.py:392
  21.1 14.6 %collective-permute-start.10 = (bf16[512,512]{1,0:T(8,128)(2,1)}, bf16[512,512]{1,0:T(8,128)(2,1)S(1)}, u32[]{:S(2)}, u32[]{:S(2)}) collective-permute-start(bf16[512,512]{1,0:T(8,128)(2,1)} %get-tuple-element.45.refs_0_), channel_id=1, source_target_pairs={{0,16},{16,32},{32,48},{48,0},{64,80},{80,96},{96,112},{112,64},{1... | collective-permute-start | bytes 1572872 | tf_op jit(solution)/shard_map/ppermute | solution.py:385
  30.5 81.8 %collective-permute-start.8 = (bf16[3,320,1024]{2,1,0:T(8,128)(2,1)S(1)}, bf16[3,320,1024]{2,1,0:T(8,128)(2,1)}, u32[]{:S(2)}, u32[]{:S(2)}) collective-permute-start(bf16[3,320,1024]{2,1,0:T(8,128)(2,1)S(1)} %shard_map.73.refs_0_), channel_id=1, source_target_pairs={{0,1},{1,0},{2,3},{3,2},{4,5},{5,4},{6,7},{7,6},{8,9},{9,8},{10,11... | collective-permute-start | bytes 5898248 | tf_op jit(solution)/shard_map/ppermute | solution.py:396
  30.6 24.0 %collective-permute-start.6 = (bf16[3,64,1024]{2,1,0:T(8,128)(2,1)S(1)}, bf16[3,64,1024]{2,1,0:T(8,128)(2,1)S(1)}, u32[]{:S(2)}, u32[]{:S(2)}) collective-permute-start(bf16[3,64,1024]{2,1,0:T(8,128)(2,1)S(1)} %collective-permute-done.2.refs_3_), channel_id=1, source_target_pairs={{0,2},{1,3},{2,4},{3,5},{4,6},{5,7},{6,8},{7,9},{8,10},{9,11},{10,... | collective-permute-start | bytes 1179656 | tf_op jit(solution)/shard_map/ppermute | solution.py:392
  30.7 22.2 %collective-permute-start.4 = (bf16[3,32,1024]{2,1,0:T(8,128)(2,1)S(1)}, bf16[3,32,1024]{2,1,0:T(8,128)(2,1)S(1)}, u32[]{:S(2)}, u32[]{:S(2)}) collective-permute-start(bf16[3,32,1024]{2,1,0:T(8,128)(2,1)S(1)} %slice.24), channel_id=1, source_target_pairs={{0,4},{1,5},{2,6},{3,7},{4,8},{5,9},{6,10},{7,11},{8,12},{9,13},{1... | collective-permute-start | bytes 589832 | tf_op jit(solution)/shard_map/ppermute | solution.py:392
  35.6 17.3 %collective-permute-start.5 = (bf16[3,32,1024]{2,1,0:T(8,128)(2,1)S(1)}, bf16[3,32,1024]{2,1,0:T(8,128)(2,1)S(1)}, u32[]{:S(2)}, u32[]{:S(2)}) collective-permute-start(bf16[3,32,1024]{2,1,0:T(8,128)(2,1)S(1)} %slice.25), channel_id=1, source_target_pairs={{0,12},{1,13},{2,14},{3,15},{4,0},{5,1},{6,2},{7,3},{8,4},{9,5},{1... | collective-permute-start | bytes 589832 | tf_op jit(solution)/shard_map/ppermute | solution.py:392
  35.7 29.0 %collective-permute-start.12 = (bf16[512,512]{1,0:T(8,128)(2,1)S(1)}, bf16[512,512]{1,0:T(8,128)(2,1)S(1)}, u32[]{:S(2)}, u32[]{:S(2)}) collective-permute-start(bf16[512,512]{1,0:T(8,128)(2,1)S(1)} %copy-done.9), channel_id=1, source_target_pairs={{0,48},{16,0},{32,16},{48,32},{64,112},{80,64},{96,80},{112,96},{1... | collective-permute-start | bytes 1572872 | tf_op jit(solution)/shard_map/ppermute | solution.py:385
  52.9 14.7 %collective-permute-start.14 = (bf16[512,512]{1,0:T(8,128)(2,1)S(1)}, bf16[512,512]{1,0:T(8,128)(2,1)S(1)}, u32[]{:S(2)}, u32[]{:S(2)}) collective-permute-start(bf16[512,512]{1,0:T(8,128)(2,1)S(1)} %copy-done.11), channel_id=1, source_target_pairs={{0,64},{16,80},{32,96},{48,112},{64,128},{80,144},{96,160},{112,17... | collective-permute-start | bytes 1572872 | tf_op jit(solution)/shard_map/ppermute | solution.py:385
  64.8 47.4 %collective-permute-start.9 = (bf16[3,192,1024]{2,1,0:T(8,128)(2,1)S(1)}, bf16[3,192,1024]{2,1,0:T(8,128)(2,1)}, u32[]{:S(2)}, u32[]{:S(2)}) collective-permute-start(bf16[3,192,1024]{2,1,0:T(8,128)(2,1)S(1)} %shard_map.74.refs_1_), channel_id=1, source_target_pairs={{0,1},{1,0},{2,3},{3,2},{4,5},{5,4},{6,7},{7,6},{8,9},{9,8},{10,11... | collective-permute-start | bytes 3538952 | tf_op jit(solution)/shard_map/ppermute | solution.py:396
  67.7 20.0 %collective-permute-start.13 = (bf16[256,512]{1,0:T(8,128)(2,1)}, bf16[256,512]{1,0:T(8,128)(2,1)}, u32[]{:S(2)}, u32[]{:S(2)}) collective-permute-start(bf16[256,512]{1,0:T(8,128)(2,1)} %slice.27), channel_id=1, source_target_pairs={{0,48},{16,0},{32,16},{48,32},{64,112},{80,64},{96,80},{112,96},{1... | collective-permute-start | bytes 786440 | tf_op jit(solution)/shard_map/ppermute | solution.py:385
  69.0 18.7 %collective-permute-start.15 = (bf16[256,512]{1,0:T(8,128)(2,1)}, bf16[256,512]{1,0:T(8,128)(2,1)}, u32[]{:S(2)}, u32[]{:S(2)}) collective-permute-start(bf16[256,512]{1,0:T(8,128)(2,1)} %slice.28), channel_id=1, source_target_pairs={{0,64},{16,80},{32,96},{48,112},{64,128},{80,144},{96,160},{112,17... | collective-permute-start | bytes 786440 | tf_op jit(solution)/shard_map/ppermute | solution.py:385
  70.4 17.2 %collective-permute-start.17 = (bf16[256,512]{1,0:T(8,128)(2,1)}, bf16[256,512]{1,0:T(8,128)(2,1)}, u32[]{:S(2)}, u32[]{:S(2)}) collective-permute-start(bf16[256,512]{1,0:T(8,128)(2,1)} %slice.29), channel_id=1, source_target_pairs={{0,192},{16,208},{32,224},{48,240},{64,0},{80,16},{96,32},{112,48}... | collective-permute-start | bytes 786440 | tf_op jit(solution)/shard_map/ppermute | solution.py:385
  99.7 21.8 %collective-permute-start.19 = (bf16[512,512]{1,0:T(8,128)(2,1)S(1)}, bf16[512,512]{1,0:T(8,128)(2,1)S(1)}, u32[]{:S(2)}, u32[]{:S(2)}) collective-permute-start(bf16[512,512]{1,0:T(8,128)(2,1)S(1)} %get-tuple-element.49), channel_id=1, source_target_pairs={{0,192},{16,208},{32,224},{48,240},{64,0},{80,16},{96,32},{112,48}... | collective-permute-start | bytes 1572872 | tf_op jit(solution)/shard_map/ppermute | solution.py:385
  102.3 19.1 %collective-permute-start.20 = (bf16[512,512]{1,0:T(8,128)(2,1)S(1)}, bf16[512,512]{1,0:T(8,128)(2,1)S(1)}, u32[]{:S(2)}, u32[]{:S(2)}) collective-permute-start(bf16[512,512]{1,0:T(8,128)(2,1)S(1)} %get-tuple-element.51), channel_id=1, source_target_pairs={{0,48},{16,0},{32,16},{48,32},{64,112},{80,64},{96,80},{112,96},{1... | collective-permute-start | bytes 1572872 | tf_op jit(solution)/shard_map/ppermute | solution.py:385
  112.3 20.4 %collective-permute-start.23 = (bf16[512,512]{1,0:T(8,128)(2,1)S(1)}, bf16[512,512]{1,0:T(8,128)(2,1)S(1)}, u32[]{:S(2)}, u32[]{:S(2)}) collective-permute-start(bf16[512,512]{1,0:T(8,128)(2,1)S(1)} %get-tuple-element.54), channel_id=1, source_target_pairs={{0,32},{16,48},{32,0},{48,16},{64,96},{80,112},{96,64},{112,80},{1... | collective-permute-start | bytes 1572872 | tf_op jit(solution)/shard_map/ppermute | solution.py:385
  148.8 16.1 %collective-permute-start.25 = (bf16[512,512]{1,0:T(8,128)(2,1)S(1)}, bf16[512,512]{1,0:T(8,128)(2,1)S(1)}, u32[]{:S(2)}, u32[]{:S(2)}) collective-permute-start(bf16[512,512]{1,0:T(8,128)(2,1)S(1)} %get-tuple-element.59), channel_id=1, source_target_pairs={{0,128},{16,144},{32,160},{48,176},{64,192},{80,208},{96,224},{112... | collective-permute-start | bytes 1572872 | tf_op jit(solution)/shard_map/ppermute | solution.py:385
  150.2 20.3 %collective-permute-start.26 = (bf16[512,512]{1,0:T(8,128)(2,1)S(1)}, bf16[512,512]{1,0:T(8,128)(2,1)S(1)}, u32[]{:S(2)}, u32[]{:S(2)}) collective-permute-start(bf16[512,512]{1,0:T(8,128)(2,1)S(1)} %get-tuple-element.60), channel_id=1, source_target_pairs={{0,64},{16,80},{32,96},{48,112},{64,128},{80,144},{96,160},{112,17... | collective-permute-start | bytes 1572872 | tf_op jit(solution)/shard_map/ppermute | solution.py:385
  150.8 19.7 %collective-permute-start.27 = (bf16[512,512]{1,0:T(8,128)(2,1)S(1)}, bf16[512,512]{1,0:T(8,128)(2,1)S(1)}, u32[]{:S(2)}, u32[]{:S(2)}) collective-permute-start(bf16[512,512]{1,0:T(8,128)(2,1)S(1)} %get-tuple-element.62), channel_id=1, source_target_pairs={{0,48},{16,0},{32,16},{48,32},{64,112},{80,64},{96,80},{112,96},{1... | collective-permute-start | bytes 1572872 | tf_op jit(solution)/shard_map/ppermute | solution.py:385
  150.8 19.7 %collective-permute-start.28 = (bf16[512,512]{1,0:T(8,128)(2,1)S(1)}, bf16[512,512]{1,0:T(8,128)(2,1)S(1)}, u32[]{:S(2)}, u32[]{:S(2)}) collective-permute-start(bf16[512,512]{1,0:T(8,128)(2,1)S(1)} %get-tuple-element.63), channel_id=1, source_target_pairs={{0,32},{16,48},{32,0},{48,16},{64,96},{80,112},{96,64},{112,80},{1... | collective-permute-start | bytes 1572872 | tf_op jit(solution)/shard_map/ppermute | solution.py:385
  175.9 14.9 %collective-permute-start.30 = (bf16[512,512]{1,0:T(8,128)(2,1)S(1)}, bf16[512,512]{1,0:T(8,128)(2,1)S(1)}, u32[]{:S(2)}, u32[]{:S(2)}) collective-permute-start(bf16[512,512]{1,0:T(8,128)(2,1)S(1)} %get-tuple-element.66), channel_id=1, source_target_pairs={{0,48},{16,0},{32,16},{48,32},{64,112},{80,64},{96,80},{112,96},{1... | collective-permute-start | bytes 1572872 | tf_op jit(solution)/shard_map/ppermute | solution.py:385
  176.6 17.4 %collective-permute-start.31 = (bf16[512,512]{1,0:T(8,128)(2,1)S(1)}, bf16[512,512]{1,0:T(8,128)(2,1)S(1)}, u32[]{:S(2)}, u32[]{:S(2)}) collective-permute-start(bf16[512,512]{1,0:T(8,128)(2,1)S(1)} %get-tuple-element.67), channel_id=1, source_target_pairs={{0,16},{16,32},{32,48},{48,0},{64,80},{80,96},{96,112},{112,64},{1... | collective-permute-start | bytes 1572872 | tf_op jit(solution)/shard_map/ppermute | solution.py:385
  178.0 21.6 %collective-permute-start.32 = (bf16[512,512]{1,0:T(8,128)(2,1)S(1)}, bf16[512,512]{1,0:T(8,128)(2,1)S(1)}, u32[]{:S(2)}, u32[]{:S(2)}) collective-permute-start(bf16[512,512]{1,0:T(8,128)(2,1)S(1)} %get-tuple-element.68), channel_id=1, source_target_pairs={{0,32},{16,48},{32,0},{48,16},{64,96},{80,112},{96,64},{112,80},{1... | collective-permute-start | bytes 1572872 | tf_op jit(solution)/shard_map/ppermute | solution.py:385
  181.3 19.1 %collective-permute-start.33 = (bf16[512,512]{1,0:T(8,128)(2,1)S(1)}, bf16[512,512]{1,0:T(8,128)(2,1)S(1)}, u32[]{:S(2)}, u32[]{:S(2)}) collective-permute-start(bf16[512,512]{1,0:T(8,128)(2,1)S(1)} %get-tuple-element.70), channel_id=1, source_target_pairs={{0,192},{16,208},{32,224},{48,240},{64,0},{80,16},{96,32},{112,48}... | collective-permute-start | bytes 1572872 | tf_op jit(solution)/shard_map/ppermute | solution.py:385
  183.4 21.4 %collective-permute-start.34 = (bf16[512,512]{1,0:T(8,128)(2,1)S(1)}, bf16[512,512]{1,0:T(8,128)(2,1)S(1)}, u32[]{:S(2)}, u32[]{:S(2)}) collective-permute-start(bf16[512,512]{1,0:T(8,128)(2,1)S(1)} %get-tuple-element.71), channel_id=1, source_target_pairs={{0,64},{16,80},{32,96},{48,112},{64,128},{80,144},{96,160},{112,17... | collective-permute-start | bytes 1572872 | tf_op jit(solution)/shard_map/ppermute | solution.py:385
  (27 other events, 251.5 us)
